TPU v7x, 32 devices: a whole 2x2x4 slice. The times are simulated.
32 devices in a mesh: ep: 8 (over z, x), tp: 4 (over y, core).
Axes of the slice: x: 2, y: 2, z: 4, core: 2. Of those that a mesh axis runs over, the one named last changes fastest.
Arguments:
- tokens: bfloat16 [1024, 4096], P('ep', 'tp'), may hold values from -6 to 6
- norm_gain: float32 [4096], replicated, may hold values from 0.1 to 1.9
- expert_ids: int32 [1024, 2], P('ep'), may hold values from 0 to 7, all different within a row; in each aligned block of 128 rows (0 to 127, 128 to 255, ...) at most 48 rows name the same one
- expert_gates: float32 [1024, 2], P('ep'), may hold values from 0.2 to 1
- gate_proj: bfloat16 [8, 4096, 512], P('ep', None, 'tp'), may hold values from -0.09375 to 0.09375
- up_proj: bfloat16 [8, 4096, 512], P('ep', None, 'tp'), may hold values from -0.09375 to 0.09375
- down_proj: bfloat16 [8, 512, 4096], P('ep', None, 'tp'), may hold values from -0.25 to 0.25
- shared_gate: bfloat16 [4096, 512], P('ep', 'tp'), may hold values from -0.09375 to 0.09375
- shared_up: bfloat16 [4096, 512], P('ep', 'tp'), may hold values from -0.09375 to 0.09375
- shared_down: bfloat16 [512, 4096], P(None, 'tp'), may hold values from -0.25 to 0.25
Outputs:
- mixed: bfloat16 [1024, 4096], P('ep', 'tp')
Inputs may be any that keep to these rules, and one draw needn't show every extreme that they name: `expert_ids`: each row names 2 distinct experts. Among the 128 rows of one index of ep (aligned blocks) no expert is named by more than 48 rows, a bound that some block reaches.
All inputs are finite; a program needn't handle non-finite values.
Results may differ from a plain program's by a relative error of at most 0.0067.
Values may be sent and summed in bfloat16 or wider, within the bound.
A program may use at most 64 MiB of HBM per device.

v0:
```python
import functools

import jax
import jax.numpy as jnp
from jax import lax
from jax.experimental import pallas as pl
from jax.experimental.pallas import tpu as pltpu
from jax.sharding import PartitionSpec as P

MESH = pl.DeviceIdType.MESH


def shards_plain(
    tokens,
    norm_gain,
    expert_ids,
    expert_gates,
    gate_proj,
    up_proj,
    down_proj,
    shared_gate,
    shared_up,
    shared_down,
):
    n_ep = lax.axis_size("ep")
    n_tp = lax.axis_size("tp")
    whole = lax.all_gather(tokens, "tp", axis=1, tiled=True)
    tok_rows, width = whole.shape
    quarter = width // n_tp
    floats = whole.astype(jnp.float32)
    scale = lax.rsqrt(jnp.mean(floats * floats, axis=-1, keepdims=True) + 1e-06)
    normed = (floats * scale * norm_gain[None, :]).astype(jnp.bfloat16)
    gate_whole, up_whole = (
        lax.all_gather(shared_gate, "ep", axis=0, tiled=True),
        lax.all_gather(shared_up, "ep", axis=0, tiled=True),
    )
    shared_g = jnp.dot(normed, gate_whole, preferred_element_type=jnp.float32)
    shared_u = jnp.dot(normed, up_whole, preferred_element_type=jnp.float32)
    shared_hidden = (jax.nn.silu(shared_g) * shared_u).astype(jnp.bfloat16)
    rows = shared_down
    shared_out = jnp.dot(
        lax.all_gather(shared_hidden, "tp", axis=1, tiled=True),
        rows,
        preferred_element_type=jnp.float32,
    )
    exp_dev = gate_proj.shape[0]
    n_exp = exp_dev * n_ep
    top = expert_ids.shape[1]
    cap = 3 * tok_rows * top // (2 * n_exp)
    flat_ids = expert_ids.reshape(tok_rows * top)
    onehot = (flat_ids[:, None] == jnp.arange(n_exp, dtype=jnp.int32)[None, :]).astype(jnp.int32)
    slots = jnp.sum((jnp.cumsum(onehot, axis=0) - onehot) * onehot, axis=-1)
    dest = flat_ids * cap + slots
    local_tok = jnp.repeat(jnp.arange(tok_rows, dtype=jnp.int32), top)
    owner = jnp.full((n_exp * cap,), tok_rows, jnp.int32).at[dest].set(local_tok)
    padded = jnp.concatenate([normed, jnp.zeros((1, width), jnp.bfloat16)], axis=0)
    outgoing = padded[owner].reshape(n_ep, exp_dev, cap, width)
    received = lax.all_to_all(outgoing, "ep", split_axis=0, concat_axis=0, tiled=True)
    gate_vals = jnp.einsum(
        "secd,edh->sech", received, gate_proj, preferred_element_type=jnp.float32
    )
    up_vals = jnp.einsum("secd,edh->sech", received, up_proj, preferred_element_type=jnp.float32)
    expert_hidden = (jax.nn.silu(gate_vals) * up_vals).astype(jnp.bfloat16)
    rows = down_proj
    expert_out = jnp.einsum(
        "sech,ehd->secd",
        lax.all_gather(expert_hidden, "tp", axis=3, tiled=True),
        rows,
        preferred_element_type=jnp.float32,
    ).astype(jnp.bfloat16)
    returned = lax.all_to_all(expert_out, "ep", split_axis=0, concat_axis=0, tiled=True)
    picked = returned.reshape(n_exp * cap, quarter)[dest].reshape(tok_rows, top, quarter)
    routed = jnp.sum(expert_gates[:, :, None] * picked.astype(jnp.float32), axis=1)
    return (routed + shared_out).astype(jnp.bfloat16)


def fits(mesh):
    return mesh.shape["tp"] == 4 and mesh.shape["ep"] % 2 == 0 and mesh.shape["ep"] <= 16


def remote(src, dst, send, recv, ep, tp):
    return pltpu.make_async_remote_copy(
        src_ref=src, dst_ref=dst, send_sem=send, recv_sem=recv, device_id=(ep, tp), device_id_type=MESH
    )


def silu_mul(v, hid):
    g, u = v[:, :hid], v[:, hid:]
    return ((g / (1.0 + jnp.exp(-g))) * u).astype(jnp.bfloat16)


def kernel(
    n,
    tokens, gain, ids, gates, gate_w, up_w, down_w, sgate_w, sup_w, sdown_w,
    out,
    wgu, wdn, sdn, pick, back, outbox, xs, own, hb, shb, ob, ret, sw, nown,
    load_sem, disp_s, disp_r, mate_s, mate_r, far_s, far_r, fwd_s, fwd_r,
    own_s, own_r, hid_s, hid_r, shid_s, shid_r, ret_s, ret_r, sw_s, sw_r, swx_s, swx_r,
):
    ep, tp = lax.axis_index("ep"), lax.axis_index("tp")
    nz = n // 2
    z, x = ep // 2, ep % 2
    ox = ep + 1 - 2 * x
    mate = tp + 1 - 2 * (tp % 2)
    far = (tp + 2) % 4
    diag = (mate + 2) % 4
    rows, quarter = tokens.shape
    cap = xs.shape[2]
    hid = gate_w.shape[2]
    slots = n * cap
    width = gain.shape[1]

    loads = [
        pltpu.make_async_copy(sgate_w, sw.at[ep, :, pl.ds(0, hid)], load_sem.at[0]),
        pltpu.make_async_copy(sup_w, sw.at[ep, :, pl.ds(hid, hid)], load_sem.at[1]),
        pltpu.make_async_copy(gate_w.at[0], wgu.at[:, pl.ds(0, hid)], load_sem.at[2]),
        pltpu.make_async_copy(up_w.at[0], wgu.at[:, pl.ds(hid, hid)], load_sem.at[3]),
        pltpu.make_async_copy(down_w.at[0], wdn, load_sem.at[4]),
        pltpu.make_async_copy(sdown_w, sdn, load_sem.at[5]),
    ]
    for c in loads:
        c.start()

    barrier = pltpu.get_barrier_semaphore()
    for d in range(1, n):
        pl.semaphore_signal(barrier, inc=1, device_id=((ep + d) % n, tp), device_id_type=MESH)
    for d in range(1, 4):
        pl.semaphore_signal(barrier, inc=1, device_id=(ep, (tp + d) % 4), device_id_type=MESH)

    lane = lax.broadcasted_iota(jnp.int32, (rows, 128), 1)
    named0 = (lane == ids[:, 0:1]).astype(jnp.float32)
    named1 = (lane == ids[:, 1:2]).astype(jnp.float32)
    named = (named0 + named1).astype(jnp.bfloat16)
    before = (
        lax.broadcasted_iota(jnp.int32, (rows, rows), 1) < lax.broadcasted_iota(jnp.int32, (rows, rows), 0)
    ).astype(jnp.float32).astype(jnp.bfloat16)
    place = jnp.dot(before, named, preferred_element_type=jnp.float32).astype(jnp.bfloat16)
    first = lax.broadcasted_iota(jnp.int32, (128, slots), 0) * cap
    col = lax.broadcasted_iota(jnp.int32, (128, slots), 1)
    spread = ((col >= first) & (col < first + cap)).astype(jnp.float32).astype(jnp.bfloat16)
    place_x = jnp.dot(place, spread, preferred_element_type=jnp.float32)
    colf = lax.broadcasted_iota(jnp.int32, (rows, slots), 1).astype(jnp.float32)
    inner = colf - jnp.floor((colf + 0.5) / cap) * cap
    hit = jnp.abs(place_x - inner) < 0.5
    total = jnp.zeros((rows, slots), jnp.float32)
    for k, one in enumerate((named0, named1)):
        sel = jnp.where(
            hit, jnp.dot(one.astype(jnp.bfloat16), spread, preferred_element_type=jnp.float32), 0.0
        )
        back[k] = sel.astype(jnp.bfloat16)
        total = total + sel
    pick[...] = total.T.astype(jnp.bfloat16)
    for e in range(n):
        outbox[e] = jnp.dot(
            pick[e * cap : (e + 1) * cap, :], tokens[...], preferred_element_type=jnp.float32
        ).astype(jnp.bfloat16)

    pl.semaphore_wait(barrier, n - 1 + 3)

    sends = []

    def go(c):
        c.start()
        sends.append(c)

    xs[tp, ep] = outbox[ep]

    def dispatch(e):
        go(remote(outbox.at[e], xs.at[tp, ep], disp_s.at[e], disp_r.at[ep], e, tp))

    for i in range(1, nz):
        for j in range(2):
            dispatch(((z + i) % nz) * 2 + (x + j) % 2)
        if i == 1:
            dispatch(ox)
            go(remote(tokens, own.at[tp], own_s.at[0], own_r.at[0], ep, mate))
            go(remote(tokens, own.at[tp], own_s.at[1], own_r.at[1], ep, far))
    if nz == 1:
        dispatch(ox)
        go(remote(tokens, own.at[tp], own_s.at[0], own_r.at[0], ep, mate))
        go(remote(tokens, own.at[tp], own_s.at[1], own_r.at[1], ep, far))
    own[tp] = tokens[...]

    loads[0].wait()
    loads[1].wait()

    def landed(dst, sem):
        return remote(dst, dst, sem, sem, ep, mate).wait_recv()

    def chain(k, way):
        s = ep - 2 * k * way
        f = (1 - way) // 2
        return remote(sw.at[s], sw.at[s], sw_s.at[f, k], sw_r.at[f, k + 1], ep + 2 * way, tp)

    def inside(zz):
        return (zz >= 0) & (zz < nz)

    def across(zz):
        s = zz * 2 + x
        return remote(sw.at[s], sw.at[s], swx_s.at[zz], swx_r.at[zz], ox, tp)

    def walk(k):
        if k == 0:
            across(z).start()
        for way in (1, -1):
            if k > 0:
                @pl.when(inside(z - k * way))
                def _():
                    s = ep - 2 * k * way
                    landed(sw.at[s], sw_r.at[(1 - way) // 2, k])
                    across(z - k * way).start()

            if k < nz - 1:
                @pl.when(inside(z - k * way) & inside(z + way))
                def _():
                    chain(k, way).start()

    def walked():
        for zz in range(nz):
            across(zz).wait_send()
        for k in range(nz - 1):
            for way in (1, -1):
                @pl.when(inside(z - k * way) & inside(z + way))
                def _():
                    chain(k, way).wait_send()

    walk(0)

    def pair(ref, k, i):
        zz = (z - i + nz) % nz
        return ref.at[k, pl.ds(zz * 2, 2)]

    def stage_a(i):
        zz = (z - i + nz) % nz
        for j in range(2):
            s = zz * 2 + j
            if i > 0:
                landed(xs.at[tp, s], disp_r.at[s])
        if i == 0:
            landed(xs.at[tp, ox], disp_r.at[ox])
        blk = pair(xs, tp, i)
        go(remote(blk, blk, far_s.at[i], far_r.at[i], ep, far))
        go(remote(blk, blk, mate_s.at[i], mate_r.at[i], ep, mate))

    def stage_b(i):
        blk = pair(xs, far, i)
        landed(blk, far_r.at[i])
        go(remote(blk, blk, fwd_s.at[i], fwd_r.at[i], ep, mate))

    def norm_scale(get, m):
        sq = jnp.zeros((m, 1), jnp.float32)
        for k in range(4):
            v = get(k).astype(jnp.float32)
            sq = sq + jnp.sum(v * v, axis=-1, keepdims=True)
        return lax.rsqrt(sq / width + 1e-06)

    def stage_c(i):
        landed(pair(xs, mate, i), mate_r.at[i])
        landed(pair(xs, diag, i), fwd_r.at[i])
        if i == 0:
            loads[2].wait()
            loads[3].wait()
        zz = (z - i + nz) % nz

        def get(k):
            return xs[k, pl.ds(zz * 2, 2)].reshape(2 * cap, quarter)

        scale = norm_scale(get, 2 * cap)
        acc = jnp.zeros((2 * cap, 2 * hid), jnp.float32)
        for k in range(4):
            cols = slice(k * quarter, (k + 1) * quarter)
            nk = (get(k).astype(jnp.float32) * scale * gain[:, cols]).astype(jnp.bfloat16)
            acc = acc + jnp.dot(nk, wgu[cols, :], preferred_element_type=jnp.float32)
        at = pl.ds(pl.multiple_of(tp * hid, 128), hid)
        hb[pl.ds(zz * 2, 2), :, at] = silu_mul(acc, hid).reshape(2, cap, hid)
        for d in range(1, 4):
            blk = hb.at[pl.ds(zz * 2, 2), :, at]
            go(remote(blk, blk, hid_s.at[i, d], hid_r.at[i, d], ep, (tp + d) % 4))

    def stage_d(i):
        zz = (z - i + nz) % nz
        for d in range(1, 4):
            at = pl.ds(pl.multiple_of(((tp - d + 4) % 4) * hid, 128), hid)
            landed(hb.at[pl.ds(zz * 2, 2), :, at], hid_r.at[i, d])
        if i == 0:
            loads[4].wait()
        h = hb[pl.ds(zz * 2, 2)].reshape(2 * cap, 4 * hid)
        res = jnp.dot(h, wdn[...], preferred_element_type=jnp.float32).astype(jnp.bfloat16)
        ob[pl.ds(zz * 2, 2)] = res.reshape(2, cap, quarter)
        for j in range(2):
            s = zz * 2 + (x + j) % 2
            if i == 0 and j == 0:
                ret[ep] = ob[ep]
            else:
                go(remote(ob.at[s], ret.at[ep], ret_s.at[s], ret_r.at[ep], s, tp))

    def own_forward():
        landed(own.at[far], own_r.at[1])
        go(remote(own.at[far], own.at[far], own_s.at[2], own_r.at[2], ep, mate))

    depth = sw.shape[1]
    per = quarter // depth

    def own_normed():
        landed(own.at[mate], own_r.at[0])
        landed(own.at[diag], own_r.at[2])
        scale = norm_scale(lambda k: own[k], rows)
        for s in range(n):
            nown[s] = (
                own[s // per, :, (s % per) * depth : (s % per + 1) * depth].astype(jnp.float32)
                * scale
                * gain[:, s * depth : (s + 1) * depth]
            ).astype(jnp.bfloat16)

    for t in range(nz + 3):
        if t < nz:
            stage_a(t)
        if t == 1:
            own_forward()
        if 0 <= t - 1 < nz:
            stage_b(t - 1)
        if 0 <= t - 2 < nz:
            stage_c(t - 2)
        if t == nz - 1 and nz > 1:
            walk(1)
        if t == nz + 1 and nz > 2:
            walk(2)
        if 0 <= t - 3 < nz:
            stage_d(t - 3)

    own_normed()
    for k in range(3 if nz > 2 else nz, nz):
        walk(k)
    acc = jnp.zeros((rows, 2 * hid), jnp.float32)
    for i in range(nz):
        s = ((z - i + nz) % nz) * 2 + x
        acc = acc + jnp.dot(nown[s], sw[s], preferred_element_type=jnp.float32)
    for i in range(nz):
        zz = (z - i + nz) % nz
        s = zz * 2 + (1 - x)
        landed(sw.at[s], swx_r.at[zz])
        acc = acc + jnp.dot(nown[s], sw[s], preferred_element_type=jnp.float32)
    at = pl.ds(pl.multiple_of(tp * hid, 128), hid)
    shb[:, at] = silu_mul(acc, hid)
    for d in range(1, 4):
        go(remote(shb.at[:, at], shb.at[:, at], shid_s.at[d], shid_r.at[d], ep, (tp + d) % 4))
    for d in range(1, 4):
        frm = pl.ds(pl.multiple_of(((tp - d + 4) % 4) * hid, 128), hid)
        landed(shb.at[:, frm], shid_r.at[d])
    loads[5].wait()
    shared = jnp.dot(shb[...], sdn[...], preferred_element_type=jnp.float32)

    for d in range(1, n):
        s = (ep + d) % n
        landed(ret.at[s], ret_r.at[s])
    got = ret[...].reshape(slots, quarter)
    mixed = shared
    for k in range(2):
        mixed = mixed + gates[:, k : k + 1] * jnp.dot(back[k], got, preferred_element_type=jnp.float32)
    out[...] = mixed.astype(jnp.bfloat16)
    for c in sends:
        c.wait_send()
    walked()


def shards(
    tokens, norm_gain, expert_ids, expert_gates, gate_proj, up_proj, down_proj,
    shared_gate, shared_up, shared_down, plain,
):
    n = lax.axis_size("ep")
    rows, quarter = tokens.shape
    top = expert_ids.shape[1]
    exp_dev = gate_proj.shape[0]
    cap = 3 * rows * top // (2 * exp_dev * n)
    hid = gate_proj.shape[2]
    ok = exp_dev == 1 and top == 2 and cap % 16 == 0 and hid % 128 == 0 and rows == 128
    ok = ok and shared_gate.shape[1] == hid and quarter % shared_gate.shape[0] == 0
    if plain or not ok:
        return shards_plain(
            tokens, norm_gain, expert_ids, expert_gates, gate_proj, up_proj, down_proj,
            shared_gate, shared_up, shared_down,
        )
    width = norm_gain.shape[0]
    bf = jnp.bfloat16
    nz = n // 2
    dma = pltpu.SemaphoreType.DMA
    vm = pl.BlockSpec(memory_space=pltpu.VMEM)
    hbm = pl.BlockSpec(memory_space=pl.ANY)
    return pl.pallas_call(
        functools.partial(kernel, n),
        out_shape=jax.ShapeDtypeStruct((rows, quarter), bf),
        in_specs=[vm] * 4 + [hbm] * 6,
        out_specs=vm,
        scratch_shapes=[
            pltpu.VMEM((width, 2 * hid), bf),
            pltpu.VMEM(down_proj.shape[1:], bf),
            pltpu.VMEM(shared_down.shape, bf),
            pltpu.VMEM((n * cap, rows), bf),
            pltpu.VMEM((2, rows, n * cap), bf),
            pltpu.VMEM((n, cap, quarter), bf),
            pltpu.VMEM((4, n, cap, quarter), bf),
            pltpu.VMEM((4, rows, quarter), bf),
            pltpu.VMEM((n, cap, 4 * hid), bf),
            pltpu.VMEM((rows, 4 * hid), bf),
            pltpu.VMEM((n, cap, quarter), bf),
            pltpu.VMEM((n, cap, quarter), bf),
            pltpu.VMEM((n, shared_gate.shape[0], 2 * hid), bf),
            pltpu.VMEM((n, rows, shared_gate.shape[0]), bf),
            dma((6,)),
            dma((n,)), dma((n,)),
            dma((nz,)), dma((nz,)),
            dma((nz,)), dma((nz,)),
            dma((nz,)), dma((nz,)),
            dma((3,)), dma((3,)),
            dma((nz, 4)), dma((nz, 4)),
            dma((4,)), dma((4,)),
            dma((n,)), dma((n,)),
            dma((2, nz)), dma((2, nz)),
            dma((nz,)), dma((nz,)),
        ],
        compiler_params=pltpu.CompilerParams(collective_id=0, has_side_effects=True, vmem_limit_bytes=48 * 1024 * 1024),
    )(tokens, norm_gain.reshape(1, width), expert_ids, expert_gates, gate_proj, up_proj, down_proj,
      shared_gate, shared_up, shared_down)


def solution(mesh):
    return jax.shard_map(
        functools.partial(shards, plain=not fits(mesh)),
        mesh=mesh,
        in_specs=(
            P("ep", "tp"),
            P(),
            P("ep", None),
            P("ep", None),
            P("ep", None, "tp"),
            P("ep", None, "tp"),
            P("ep", None, "tp"),
            P("ep", "tp"),
            P("ep", "tp"),
            P(None, "tp"),
        ),
        out_specs=P("ep", "tp"),
        check_vma=False,
    )
```

profile of v0, /device:TPU:0, one launch (start us, length us, event | category | flops | bytes accessed | tf_op | source)
XLA Modules:
  0.0 74.4 jit_solution(18357203503654468268)
XLA Ops:
  0.0 0.0 copy-start.5
  0.0 0.8 %copy.11.ids = s32[128,2]{1,0:T(8,128)S(1)} copy(s32[128,2]{0,1:T(2,128)} %param.12) | data formatting | bytes 2048 | tf_op args[2]
  0.8 0.8 %copy.12.gates = f32[128,2]{1,0:T(8,128)S(1)} copy(f32[128,2]{0,1:T(2,128)} %param.13) | data formatting | bytes 2048 | tf_op args[3]
  1.6 0.0 copy-done.5
  1.6 0.0 copy-start
  1.6 1.2 %copy-done = bf16[1,4096,128]{2,1,0:T(8,128)(2,1)S(1)} copy-done((bf16[1,4096,128]{2,1,0:T(8,128)(2,1)S(1)}, bf16[1,4096,128]{2,1,0:T(8,128)(2,1)}, u32[]{:S(2)}) %copy-start) | copy-done | bytes 1048600
  2.8 0.0 copy-start.1
  2.8 1.2 %copy-done.1 = bf16[1,4096,128]{2,1,0:T(8,128)(2,1)S(1)} copy-done((bf16[1,4096,128]{2,1,0:T(8,128)(2,1)S(1)}, bf16[1,4096,128]{2,1,0:T(8,128)(2,1)}, u32[]{:S(2)}) %copy-start.1) | copy-done | bytes 1048600
  4.1 0.0 copy-start.2
  4.1 1.2 %copy-done.2 = bf16[1,512,1024]{2,1,0:T(8,128)(2,1)S(1)} copy-done((bf16[1,512,1024]{2,1,0:T(8,128)(2,1)S(1)}, bf16[1,512,1024]{2,1,0:T(8,128)(2,1)}, u32[]{:S(2)}) %copy-start.2) | copy-done | bytes 1048600
  5.3 0.0 copy-start.3
  5.3 1.2 %copy-done.3 = bf16[512,1024]{1,0:T(8,128)(2,1)S(1)} copy-done((bf16[512,1024]{1,0:T(8,128)(2,1)S(1)}, bf16[512,1024]{1,0:T(8,128)(2,1)}, u32[]{:S(2)}) %copy-start.3) | copy-done | bytes 1048600
  6.5 0.0 copy-start.4
  6.5 0.9 %copy-done.4 = bf16[128,1024]{1,0:T(8,128)(2,1)S(1)} copy-done((bf16[128,1024]{1,0:T(8,128)(2,1)S(1)}, bf16[128,1024]{1,0:T(8,128)(2,1)}, u32[]{:S(2)}) %copy-start.4) | copy-done | bytes 262168
  7.5 0.0 copy-start.6
  7.5 0.9 %copy-done.6 = bf16[512,128]{1,0:T(8,128)(2,1)S(1)} copy-done((bf16[512,128]{1,0:T(8,128)(2,1)S(1)}, bf16[512,128]{1,0:T(8,128)(2,1)}, u32[]{:S(2)}) %copy-start.6) | copy-done | bytes 131096
  8.4 0.0 copy-start.7
  8.4 0.7 copy-done.7
  9.1 64.6 %shard_map.100 = bf16[128,1024]{1,0:T(8,128)(2,1)S(1)} custom-call(bf16[128,1024]{1,0:T(8,128)(2,1)S(1)} %copy-done.4, f32[1,4096]{1,0:T(1,128)S(1)} %bitcast.1, s32[128,2]{1,0:T(8,128)S(1)} %copy.11.ids, f32[128,2]{1,0:T(8,128)S(1)} %copy.12.gates, bf16[1,4096,128]{2,1,0:T(8,128)(2,1)S(1)} %copy-done, bf16[1,4096,128]{2,1,0:T(8,128)(2,1)S(1)} %copy-done.1, ...), custom_call_target="tpu_custom_call" | custom-call | tf_op jit(solution)/shard_map/pallas_call | solution.py:389
  73.7 0.7 copy.14
Async XLA Ops:
  0.0 1.6 %copy-start.5 = (bf16[512,128]{1,0:T(8,128)(2,1)S(1)}, bf16[512,128]{1,0:T(8,128)(2,1)}, u32[]{:S(2)}) copy-start(bf16[512,128]{1,0:T(8,128)(2,1)} %sgate_w.1) | copy-start | bytes 393220
  1.6 1.2 %copy-start = (bf16[1,4096,128]{2,1,0:T(8,128)(2,1)S(1)}, bf16[1,4096,128]{2,1,0:T(8,128)(2,1)}, u32[]{:S(2)}) copy-start(bf16[1,4096,128]{2,1,0:T(8,128)(2,1)} %gate_w.1) | copy-start | bytes 3145732
  2.8 1.2 %copy-start.1 = (bf16[1,4096,128]{2,1,0:T(8,128)(2,1)S(1)}, bf16[1,4096,128]{2,1,0:T(8,128)(2,1)}, u32[]{:S(2)}) copy-start(bf16[1,4096,128]{2,1,0:T(8,128)(2,1)} %up_w.1) | copy-start | bytes 3145732
  4.1 1.2 %copy-start.2 = (bf16[1,512,1024]{2,1,0:T(8,128)(2,1)S(1)}, bf16[1,512,1024]{2,1,0:T(8,128)(2,1)}, u32[]{:S(2)}) copy-start(bf16[1,512,1024]{2,1,0:T(8,128)(2,1)} %down_w.1) | copy-start | bytes 3145732
  5.3 1.2 %copy-start.3 = (bf16[512,1024]{1,0:T(8,128)(2,1)S(1)}, bf16[512,1024]{1,0:T(8,128)(2,1)}, u32[]{:S(2)}) copy-start(bf16[512,1024]{1,0:T(8,128)(2,1)} %sdown_w.1) | copy-start | bytes 3145732
  6.5 0.9 %copy-start.4 = (bf16[128,1024]{1,0:T(8,128)(2,1)S(1)}, bf16[128,1024]{1,0:T(8,128)(2,1)}, u32[]{:S(2)}) copy-start(bf16[128,1024]{1,0:T(8,128)(2,1)} %tokens.1) | copy-start | bytes 786436
  7.5 0.9 %copy-start.6 = (bf16[512,128]{1,0:T(8,128)(2,1)S(1)}, bf16[512,128]{1,0:T(8,128)(2,1)}, u32[]{:S(2)}) copy-start(bf16[512,128]{1,0:T(8,128)(2,1)} %sup_w.1) | copy-start | bytes 393220
  8.4 0.7 copy-start.7
where the time goes:
time: 75.4 us; the launch traced here: 74.4 us
  Pallas kernels  64.6 us (86%)
  local copies, waits for them, and re-layouts  9.78 us (13%)
    pallas_call x1, Pallas kernels, shards(): pl.pallas_call(functools.partial(kernel, n), out_shape=jax.ShapeDtypeStru...  64.6 us
    unnamed x19, local copies, waits for them, and re-layouts  9.78 us

commit v1 on v0

--- a/solution.py
+++ b/solution.py
@@ -91,9 +91,9 @@
 
 def kernel(
     n,
-    tokens, gain, ids, gates, gate_w, up_w, down_w, sgate_w, sup_w, sdown_w,
+    tokens_hbm, gain_hbm, ids_hbm, gates_hbm, gate_w, up_w, down_w, sgate_w, sup_w, sdown_w,
     out,
-    wgu, wdn, sdn, pick, back, outbox, xs, own, hb, shb, ob, ret, sw, nown,
+    tokens, gain, ids, gates, wgu, wdn, sdn, pick, back, outbox, xs, own, hb, shb, ob, ret, sw, nown,
     load_sem, disp_s, disp_r, mate_s, mate_r, far_s, far_r, fwd_s, fwd_r,
     own_s, own_r, hid_s, hid_r, shid_s, shid_r, ret_s, ret_r, sw_s, sw_r, swx_s, swx_r,
 ):
@@ -110,6 +110,14 @@
     slots = n * cap
     width = gain.shape[1]
 
+    first = [
+        pltpu.make_async_copy(ids_hbm, ids, load_sem.at[6]),
+        pltpu.make_async_copy(tokens_hbm, tokens, load_sem.at[7]),
+        pltpu.make_async_copy(gates_hbm, gates, load_sem.at[8]),
+        pltpu.make_async_copy(gain_hbm, gain, load_sem.at[9]),
+    ]
+    for c in first:
+        c.start()
     loads = [
         pltpu.make_async_copy(sgate_w, sw.at[ep, :, pl.ds(0, hid)], load_sem.at[0]),
         pltpu.make_async_copy(sup_w, sw.at[ep, :, pl.ds(hid, hid)], load_sem.at[1]),
@@ -127,17 +135,21 @@
     for d in range(1, 4):
         pl.semaphore_signal(barrier, inc=1, device_id=(ep, (tp + d) % 4), device_id_type=MESH)
 
-    lane = lax.broadcasted_iota(jnp.int32, (rows, 128), 1)
-    named0 = (lane == ids[:, 0:1]).astype(jnp.float32)
-    named1 = (lane == ids[:, 1:2]).astype(jnp.float32)
+    def column(row):
+        return jnp.broadcast_to(row.astype(jnp.float32), (rows, rows)).T
+
+    lane = lax.broadcasted_iota(jnp.int32, (rows, 128), 1).astype(jnp.float32)
+    first[0].wait()
+    named0 = (lane == column(ids[0:1, :])).astype(jnp.float32)
+    named1 = (lane == column(ids[1:2, :])).astype(jnp.float32)
     named = (named0 + named1).astype(jnp.bfloat16)
     before = (
         lax.broadcasted_iota(jnp.int32, (rows, rows), 1) < lax.broadcasted_iota(jnp.int32, (rows, rows), 0)
     ).astype(jnp.float32).astype(jnp.bfloat16)
     place = jnp.dot(before, named, preferred_element_type=jnp.float32).astype(jnp.bfloat16)
-    first = lax.broadcasted_iota(jnp.int32, (128, slots), 0) * cap
+    low = lax.broadcasted_iota(jnp.int32, (128, slots), 0) * cap
     col = lax.broadcasted_iota(jnp.int32, (128, slots), 1)
-    spread = ((col >= first) & (col < first + cap)).astype(jnp.float32).astype(jnp.bfloat16)
+    spread = ((col >= low) & (col < low + cap)).astype(jnp.float32).astype(jnp.bfloat16)
     place_x = jnp.dot(place, spread, preferred_element_type=jnp.float32)
     colf = lax.broadcasted_iota(jnp.int32, (rows, slots), 1).astype(jnp.float32)
     inner = colf - jnp.floor((colf + 0.5) / cap) * cap
@@ -150,6 +162,7 @@
         back[k] = sel.astype(jnp.bfloat16)
         total = total + sel
     pick[...] = total.T.astype(jnp.bfloat16)
+    first[1].wait()
     for e in range(n):
         outbox[e] = jnp.dot(
             pick[e * cap : (e + 1) * cap, :], tokens[...], preferred_element_type=jnp.float32
@@ -260,6 +273,7 @@
         if i == 0:
             loads[2].wait()
             loads[3].wait()
+            first[3].wait()
         zz = (z - i + nz) % nz
 
         def get(k):
@@ -355,8 +369,9 @@
         landed(ret.at[s], ret_r.at[s])
     got = ret[...].reshape(slots, quarter)
     mixed = shared
+    first[2].wait()
     for k in range(2):
-        mixed = mixed + gates[:, k : k + 1] * jnp.dot(back[k], got, preferred_element_type=jnp.float32)
+        mixed = mixed + column(gates[k : k + 1, :])[:, 0:1] * jnp.dot(back[k], got, preferred_element_type=jnp.float32)
     out[...] = mixed.astype(jnp.bfloat16)
     for c in sends:
         c.wait_send()
@@ -385,13 +400,17 @@
     nz = n // 2
     dma = pltpu.SemaphoreType.DMA
     vm = pl.BlockSpec(memory_space=pltpu.VMEM)
-    hbm = pl.BlockSpec(memory_space=pl.ANY)
+    hbm = pl.BlockSpec(memory_space=pltpu.HBM)
     return pl.pallas_call(
         functools.partial(kernel, n),
         out_shape=jax.ShapeDtypeStruct((rows, quarter), bf),
-        in_specs=[vm] * 4 + [hbm] * 6,
+        in_specs=[hbm] * 10,
         out_specs=vm,
         scratch_shapes=[
+            pltpu.VMEM(tokens.shape, bf),
+            pltpu.VMEM((1, width), jnp.float32),
+            pltpu.VMEM((top, rows), jnp.int32),
+            pltpu.VMEM((top, rows), jnp.float32),
             pltpu.VMEM((width, 2 * hid), bf),
             pltpu.VMEM(down_proj.shape[1:], bf),
             pltpu.VMEM(shared_down.shape, bf),
@@ -406,7 +425,7 @@
             pltpu.VMEM((n, cap, quarter), bf),
             pltpu.VMEM((n, shared_gate.shape[0], 2 * hid), bf),
             pltpu.VMEM((n, rows, shared_gate.shape[0]), bf),
-            dma((6,)),
+            dma((10,)),
             dma((n,)), dma((n,)),
             dma((nz,)), dma((nz,)),
             dma((nz,)), dma((nz,)),
@@ -418,8 +437,8 @@
             dma((2, nz)), dma((2, nz)),
             dma((nz,)), dma((nz,)),
         ],
-        compiler_params=pltpu.CompilerParams(collective_id=0, has_side_effects=True, vmem_limit_bytes=48 * 1024 * 1024),
-    )(tokens, norm_gain.reshape(1, width), expert_ids, expert_gates, gate_proj, up_proj, down_proj,
+        compiler_params=pltpu.CompilerParams(collective_id=0, has_side_effects=True, vmem_limit_bytes=67043328),
+    )(tokens, norm_gain.reshape(1, width), expert_ids.T, expert_gates.T, gate_proj, up_proj, down_proj,
       shared_gate, shared_up, shared_down)
 
 

time: 75.4 us -> 66.3 us (0.88)
  local copies, waits for them, and re-layouts: 9.78 us -> 1.67 us
    unnamed x19 -> x1, local copies, waits for them, and re-layouts: 9.78 us -> 1.67 us
where the time goes in v1:
time: 66.3 us; the launch traced here: 65.8 us
  Pallas kernels  64.1 us (97%)
  local copies, waits for them, and re-layouts  1.67 us (3%)
    pallas_call x1, Pallas kernels, shards(): pl.pallas_call(functools.partial(kernel, n), out_shape=jax.ShapeDtypeStru...  64.1 us
    unnamed x1, local copies, waits for them, and re-layouts  1.67 us

profile of v1, /device:TPU:0, one launch (start us, length us, event | category | flops | bytes accessed | tf_op | source)
XLA Modules:
  0.0 65.8 jit_solution(15086288468726094955)
XLA Ops:
  0.0 64.1 %shard_map.100 = bf16[128,1024]{1,0:T(8,128)(2,1)} custom-call(bf16[128,1024]{1,0:T(8,128)(2,1)} %tokens_hbm.1, f32[1,4096]{1,0:T(1,128)} %bitcast.3, s32[2,128]{1,0:T(2,128)} %bitcast.4, f32[2,128]{1,0:T(2,128)} %bitcast.5, bf16[1,4096,128]{2,1,0:T(8,128)(2,1)} %gate_w.1, bf16[1,4096,128]{2,1,0:T(8,128)(2,1)} %up_w.1, bf16[1,512,1024]{2,1,0:T(8,128)(2,1)} %down_w.1, ...), custom_call_target="tpu_custom_call" | custom-call | tf_op jit(solution)/shard_map/pallas_call | solution.py:404
  64.1 1.7 %copy.12 = bf16[128,1024]{1,0:T(8,128)(2,1)} copy(bf16[128,1024]{1,0:T(8,128)(2,1)} %shard_map.100) | data formatting | bytes 524288

commit v2 on v1

v2 whole, which is shorter than its diff:
```python
import functools

import jax
import jax.numpy as jnp
from jax import lax
from jax.experimental import pallas as pl
from jax.experimental.pallas import tpu as pltpu
from jax.sharding import PartitionSpec as P

MESH = pl.DeviceIdType.MESH


def shards_plain(
    tokens,
    norm_gain,
    expert_ids,
    expert_gates,
    gate_proj,
    up_proj,
    down_proj,
    shared_gate,
    shared_up,
    shared_down,
):
    n_ep = lax.axis_size("ep")
    n_tp = lax.axis_size("tp")
    whole = lax.all_gather(tokens, "tp", axis=1, tiled=True)
    tok_rows, width = whole.shape
    quarter = width // n_tp
    floats = whole.astype(jnp.float32)
    scale = lax.rsqrt(jnp.mean(floats * floats, axis=-1, keepdims=True) + 1e-06)
    normed = (floats * scale * norm_gain[None, :]).astype(jnp.bfloat16)
    gate_whole, up_whole = (
        lax.all_gather(shared_gate, "ep", axis=0, tiled=True),
        lax.all_gather(shared_up, "ep", axis=0, tiled=True),
    )
    shared_g = jnp.dot(normed, gate_whole, preferred_element_type=jnp.float32)
    shared_u = jnp.dot(normed, up_whole, preferred_element_type=jnp.float32)
    shared_hidden = (jax.nn.silu(shared_g) * shared_u).astype(jnp.bfloat16)
    rows = shared_down
    shared_out = jnp.dot(
        lax.all_gather(shared_hidden, "tp", axis=1, tiled=True),
        rows,
        preferred_element_type=jnp.float32,
    )
    exp_dev = gate_proj.shape[0]
    n_exp = exp_dev * n_ep
    top = expert_ids.shape[1]
    cap = 3 * tok_rows * top // (2 * n_exp)
    flat_ids = expert_ids.reshape(tok_rows * top)
    onehot = (flat_ids[:, None] == jnp.arange(n_exp, dtype=jnp.int32)[None, :]).astype(jnp.int32)
    slots = jnp.sum((jnp.cumsum(onehot, axis=0) - onehot) * onehot, axis=-1)
    dest = flat_ids * cap + slots
    local_tok = jnp.repeat(jnp.arange(tok_rows, dtype=jnp.int32), top)
    owner = jnp.full((n_exp * cap,), tok_rows, jnp.int32).at[dest].set(local_tok)
    padded = jnp.concatenate([normed, jnp.zeros((1, width), jnp.bfloat16)], axis=0)
    outgoing = padded[owner].reshape(n_ep, exp_dev, cap, width)
    received = lax.all_to_all(outgoing, "ep", split_axis=0, concat_axis=0, tiled=True)
    gate_vals = jnp.einsum(
        "secd,edh->sech", received, gate_proj, preferred_element_type=jnp.float32
    )
    up_vals = jnp.einsum("secd,edh->sech", received, up_proj, preferred_element_type=jnp.float32)
    expert_hidden = (jax.nn.silu(gate_vals) * up_vals).astype(jnp.bfloat16)
    rows = down_proj
    expert_out = jnp.einsum(
        "sech,ehd->secd",
        lax.all_gather(expert_hidden, "tp", axis=3, tiled=True),
        rows,
        preferred_element_type=jnp.float32,
    ).astype(jnp.bfloat16)
    returned = lax.all_to_all(expert_out, "ep", split_axis=0, concat_axis=0, tiled=True)
    picked = returned.reshape(n_exp * cap, quarter)[dest].reshape(tok_rows, top, quarter)
    routed = jnp.sum(expert_gates[:, :, None] * picked.astype(jnp.float32), axis=1)
    return (routed + shared_out).astype(jnp.bfloat16)


def fits(mesh):
    return mesh.shape["tp"] == 4 and mesh.shape["ep"] == 8


def remote(src, dst, send, recv, ep, tp):
    return pltpu.make_async_remote_copy(
        src_ref=src, dst_ref=dst, send_sem=send, recv_sem=recv, device_id=(ep, tp), device_id_type=MESH
    )


def silu_mul(v, hid):
    g, u = v[:, :hid], v[:, hid:]
    return ((g / (1.0 + jnp.exp(-g))) * u).astype(jnp.bfloat16)


def kernel(
    n,
    tokens_hbm, gain_hbm, ids_hbm, gates_hbm, gate_w, up_w, down_w, sgate_w, sup_w, sdown_w,
    out,
    tokens, gain, ids, gates, wgu, wdn, sdn, pick, back, outbox, xs, tk, ssq, hb, shb, ob, ret, sw,
    acc, pin, mix,
    load_sem, disp_s, disp_r, mate_s, mate_r, far_s, far_r, fwd_s, fwd_r,
    tk_s, tk_r, ssq_s, ssq_r, hid_s, hid_r, shid_s, shid_r, ret_s, ret_r, sw_s, sw_r, part_s, part_r,
):
    ep, tp = lax.axis_index("ep"), lax.axis_index("tp")
    nz = n // 2
    z, x = ep // 2, ep % 2
    ox = ep + 1 - 2 * x
    mate = tp + 1 - 2 * (tp % 2)
    far = (tp + 2) % 4
    diag = (mate + 2) % 4
    rows, quarter = tokens.shape
    cap = xs.shape[2]
    hid = gate_w.shape[2]
    slots = n * cap
    width = gain.shape[1]
    depth = sgate_w.shape[0]

    side = 1 - 2 * (z // 2)
    inner = ((z + 1) // 2) % 2
    order = [z + side * (i - inner * (0, 0, 3, 1)[i]) for i in range(nz)]

    def load(src, dst, k):
        c = pltpu.make_async_copy(src, dst, load_sem.at[k])
        c.start()
        return c

    ids_in = load(ids_hbm, ids, 0)
    tokens_in = load(tokens_hbm, tokens, 1)
    gates_in = load(gates_hbm, gates, 2)
    gain_in = load(gain_hbm, gain, 3)
    shared_in = [
        load(sgate_w, sw.at[z, :, pl.ds(0, hid)], 4),
        load(sup_w, sw.at[z, :, pl.ds(hid, hid)], 5),
    ]
    expert_in = [
        load(gate_w.at[0], wgu.at[:, pl.ds(0, hid)], 6),
        load(up_w.at[0], wgu.at[:, pl.ds(hid, hid)], 7),
    ]
    down_in = load(down_w.at[0], wdn, 8)
    sdown_in = load(sdown_w, sdn, 9)

    barrier = pltpu.get_barrier_semaphore()
    for d in range(1, n):
        pl.semaphore_signal(barrier, inc=1, device_id=((ep + d) % n, tp), device_id_type=MESH)
    for d in range(1, 4):
        pl.semaphore_signal(barrier, inc=1, device_id=(ep, (tp + d) % 4), device_id_type=MESH)

    def column(row):
        return jnp.broadcast_to(row.astype(jnp.float32), (rows, rows)).T

    lane = lax.broadcasted_iota(jnp.int32, (rows, 128), 1).astype(jnp.float32)
    ids_in.wait()
    named0 = (lane == column(ids[0:1, :])).astype(jnp.float32)
    named1 = (lane == column(ids[1:2, :])).astype(jnp.float32)
    named = (named0 + named1).astype(jnp.bfloat16)
    before = (
        lax.broadcasted_iota(jnp.int32, (rows, rows), 1) < lax.broadcasted_iota(jnp.int32, (rows, rows), 0)
    ).astype(jnp.float32).astype(jnp.bfloat16)
    place = jnp.dot(before, named, preferred_element_type=jnp.float32).astype(jnp.bfloat16)
    low = lax.broadcasted_iota(jnp.int32, (128, slots), 0) * cap
    col = lax.broadcasted_iota(jnp.int32, (128, slots), 1)
    spread = ((col >= low) & (col < low + cap)).astype(jnp.float32).astype(jnp.bfloat16)
    place_x = jnp.dot(place, spread, preferred_element_type=jnp.float32)
    colf = lax.broadcasted_iota(jnp.int32, (rows, slots), 1).astype(jnp.float32)
    within = colf - jnp.floor((colf + 0.5) / cap) * cap
    hit = jnp.abs(place_x - within) < 0.5
    total = jnp.zeros((rows, slots), jnp.float32)
    for k, one in enumerate((named0, named1)):
        sel = jnp.where(
            hit, jnp.dot(one.astype(jnp.bfloat16), spread, preferred_element_type=jnp.float32), 0.0
        )
        for e in range(nz):
            back[k, e] = sel[:, 2 * e * cap : 2 * (e + 1) * cap].astype(jnp.bfloat16)
        total = total + sel
    pick[...] = total.T.astype(jnp.bfloat16)
    tokens_in.wait()
    for e in range(n):
        outbox[e] = jnp.dot(
            pick[e * cap : (e + 1) * cap, :], tokens[...], preferred_element_type=jnp.float32
        ).astype(jnp.bfloat16)
    own = tokens[...].astype(jnp.float32)
    sums = jnp.broadcast_to(jnp.sum(own * own, axis=-1, keepdims=True), (rows, 128)).T
    ssq[tp] = sums[0:8, :]

    pl.semaphore_wait(barrier, n - 1 + 3)

    sends = []

    def go(c):
        c.start()
        sends.append(c)

    def landed(dst, sem):
        remote(dst, dst, sem, sem, ep, mate).wait_recv()

    xs[tp, ep] = outbox[ep]

    def dispatch(e):
        go(remote(outbox.at[e], xs.at[tp, ep], disp_s.at[e], disp_r.at[ep], e, tp))

    dispatch(ox)
    for i in range(1, nz):
        for j in range(2):
            dispatch(order[i] * 2 + (x + j) % 2)

    mine = tokens.at[:, pl.ds(pl.multiple_of(x * depth, depth), depth)]
    theirs = tokens.at[:, pl.ds(pl.multiple_of((1 - x) * depth, depth), depth)]
    go(remote(mine, tk.at[tp, 0], tk_s.at[0], tk_r.at[0], ep, mate))
    go(remote(mine, tk.at[tp, 0], tk_s.at[1], tk_r.at[1], ep, far))
    go(remote(theirs, tk.at[tp, 1], tk_s.at[2], tk_r.at[2], ox, tp))
    for d in range(1, 4):
        go(remote(ssq.at[tp], ssq.at[tp], ssq_s.at[d], ssq_r.at[d], ep, (tp + d) % 4))
    tk[tp, 0] = mine[...]

    def other_tokens():
        landed(tk.at[tp, 1], tk_r.at[2])
        go(remote(tk.at[tp, 1], tk.at[tp, 1], tk_s.at[3], tk_r.at[3], ep, mate))
        go(remote(tk.at[tp, 1], tk.at[tp, 1], tk_s.at[4], tk_r.at[4], ep, far))

    def pass_tokens():
        landed(tk.at[far, 0], tk_r.at[1])
        landed(tk.at[far, 1], tk_r.at[4])
        go(remote(tk.at[far], tk.at[far], tk_s.at[5], tk_r.at[5], ep, mate))

    def have_tokens():
        landed(tk.at[mate, 0], tk_r.at[0])
        landed(tk.at[mate, 1], tk_r.at[3])
        landed(tk.at[diag], tk_r.at[5])

    def pair(ref, k, i):
        return ref.at[k, pl.ds(order[i] * 2, 2)]

    def stage_a(i):
        for j in range(2):
            s = order[i] * 2 + (x + j) % 2
            blk = xs.at[tp, s]
            if i > 0 or j > 0:
                landed(blk, disp_r.at[s])
            go(remote(blk, blk, far_s.at[i, j], far_r.at[i, j], ep, far))
            go(remote(blk, blk, mate_s.at[i, j], mate_r.at[i, j], ep, mate))

    def both(k, sem, i):
        for j in range(2):
            landed(xs.at[k, order[i] * 2 + (x + j) % 2], sem.at[i, j])

    def stage_b(i):
        both(far, far_r, i)
        blk = pair(xs, far, i)
        go(remote(blk, blk, fwd_s.at[i], fwd_r.at[i], ep, mate))

    def stage_c(i):
        both(mate, mate_r, i)
        landed(pair(xs, diag, i), fwd_r.at[i])
        if i == 0:
            expert_in[0].wait()
            expert_in[1].wait()
            gain_in.wait()
        zz = order[i]
        sq = jnp.zeros((2 * cap, 1), jnp.float32)
        for k in range(4):
            v = xs[k, pl.ds(zz * 2, 2)].reshape(2 * cap, quarter).astype(jnp.float32)
            sq = sq + jnp.sum(v * v, axis=-1, keepdims=True)
        scale = lax.rsqrt(sq / width + 1e-06)
        val = jnp.zeros((2 * cap, 2 * hid), jnp.float32)
        for k in range(4):
            cols = slice(k * quarter, (k + 1) * quarter)
            v = xs[k, pl.ds(zz * 2, 2)].reshape(2 * cap, quarter).astype(jnp.float32)
            nk = (v * scale * gain[:, cols]).astype(jnp.bfloat16)
            val = val + jnp.dot(nk, wgu[cols, :], preferred_element_type=jnp.float32)
        at = pl.ds(pl.multiple_of(tp * hid, 128), hid)
        hb[pl.ds(zz * 2, 2), :, at] = silu_mul(val, hid).reshape(2, cap, hid)
        for d in (2, 1, 3):
            blk = hb.at[pl.ds(zz * 2, 2), :, at]
            go(remote(blk, blk, hid_s.at[i, d], hid_r.at[i, d], ep, (tp + d) % 4))

    def stage_d(i):
        zz = order[i]
        for d in range(1, 4):
            at = pl.ds(pl.multiple_of(((tp - d + 4) % 4) * hid, 128), hid)
            landed(hb.at[pl.ds(zz * 2, 2), :, at], hid_r.at[i, d])
        if i == 0:
            down_in.wait()
        h = hb[pl.ds(zz * 2, 2)].reshape(2 * cap, 4 * hid)
        res = jnp.dot(h, wdn[...], preferred_element_type=jnp.float32).astype(jnp.bfloat16)
        ob[pl.ds(zz * 2, 2)] = res.reshape(2, cap, quarter)
        for j in range(2):
            s = zz * 2 + (x + j) % 2
            if i == 0 and j == 0:
                ret[ep] = ob[ep]
            else:
                go(remote(ob.at[s], ret.at[ep], ret_s.at[s], ret_r.at[ep], s, tp))

    def rows_of(i, way, k):
        blk = sw.at[order[i]]
        return remote(blk, blk, sw_s.at[k], sw_r.at[order[i]], ep + 2 * way * side, tp)

    chain = [(0, 1, 0), (0, -1, 1), (1, -1, 2), (2, 1, 3), (3, -1, 4)]

    def rows_start(i):
        if i == 0:
            for c in shared_in:
                c.wait()
            rows_of(*chain[0]).start()

            @pl.when(inner == 1)
            def _():
                rows_of(*chain[1]).start()
        else:
            landed(sw.at[order[i]], sw_r.at[order[i]])

            @pl.when(inner == 1)
            def _():
                rows_of(*chain[i + 1]).start()

    def rows_end():
        rows_of(*chain[0]).wait_send()

        @pl.when(inner == 1)
        def _():
            for c in chain[1:]:
                rows_of(*c).wait_send()

    def shared_add(i):
        zz = order[i]
        cols = pl.ds(pl.multiple_of((2 * zz + x) * depth, depth), depth)
        v = (tk[zz].reshape(2 * rows, depth).astype(jnp.float32) * gain[:, cols]).astype(jnp.bfloat16)
        part = jnp.dot(v, sw[zz], preferred_element_type=jnp.float32)
        acc[...] = part if i == 0 else acc[...] + part

    def combine(i):
        zz = order[i]
        for j in range(2):
            s = zz * 2 + (x + j) % 2
            if i > 0 or j > 0:
                landed(ret.at[s], ret_r.at[s])
        got = ret[pl.ds(zz * 2, 2)].reshape(2 * cap, quarter)
        for k in range(2):
            mix[...] += column(gates[k : k + 1, :])[:, 0:1] * jnp.dot(
                back[k, zz], got, preferred_element_type=jnp.float32
            )

    stage_a(0)
    stage_a(1)
    stage_b(0)
    other_tokens()
    stage_c(0)
    stage_b(1)
    stage_a(2)
    rows_start(0)
    stage_d(0)
    stage_c(1)
    stage_d(1)
    stage_b(2)
    stage_a(3)
    pass_tokens()
    stage_c(2)
    rows_start(1)
    stage_b(3)
    stage_d(2)
    stage_c(3)
    stage_d(3)
    have_tokens()
    shared_add(0)
    shared_add(1)
    rows_start(2)
    shared_add(2)
    rows_start(3)
    shared_add(3)
    go(remote(acc.at[pl.ds(rows, rows)], pin, part_s, part_r, ox, tp))
    square = ssq[tp]
    for d in range(1, 4):
        frm = (tp - d + 4) % 4
        landed(ssq.at[frm], ssq_r.at[d])
        square = square + ssq[frm]
    scale = column(lax.rsqrt(square[0:1, :] / width + 1e-06))[:, 0:1]
    mix[...] = jnp.zeros((rows, quarter), jnp.float32)
    gates_in.wait()
    combine(0)
    landed(pin, part_r)
    at = pl.ds(pl.multiple_of(tp * hid, 128), hid)
    shb[:, at] = silu_mul((acc[0:rows, :] + pin[...]) * scale, hid)
    for d in (2, 1, 3):
        go(remote(shb.at[:, at], shb.at[:, at], shid_s.at[d], shid_r.at[d], ep, (tp + d) % 4))
    combine(1)
    combine(2)
    for d in range(1, 4):
        frm = pl.ds(pl.multiple_of(((tp - d + 4) % 4) * hid, 128), hid)
        landed(shb.at[:, frm], shid_r.at[d])
    sdown_in.wait()
    mix[...] += jnp.dot(shb[...], sdn[...], preferred_element_type=jnp.float32)
    combine(3)
    out[...] = mix[...].astype(jnp.bfloat16)
    for c in sends:
        c.wait_send()
    rows_end()


def shards(
    tokens, norm_gain, expert_ids, expert_gates, gate_proj, up_proj, down_proj,
    shared_gate, shared_up, shared_down, plain,
):
    n = lax.axis_size("ep")
    rows, quarter = tokens.shape
    top = expert_ids.shape[1]
    exp_dev = gate_proj.shape[0]
    cap = 3 * rows * top // (2 * exp_dev * n)
    hid = gate_proj.shape[2]
    depth = shared_gate.shape[0]
    ok = exp_dev == 1 and top == 2 and cap % 16 == 0 and hid % 128 == 0 and rows == 128
    ok = ok and shared_gate.shape[1] == hid and quarter == 2 * depth and depth % 128 == 0
    if plain or not ok:
        return shards_plain(
            tokens, norm_gain, expert_ids, expert_gates, gate_proj, up_proj, down_proj,
            shared_gate, shared_up, shared_down,
        )
    width = norm_gain.shape[0]
    bf = jnp.bfloat16
    nz = n // 2
    dma = pltpu.SemaphoreType.DMA
    vm = pl.BlockSpec(memory_space=pltpu.VMEM)
    hbm = pl.BlockSpec(memory_space=pltpu.HBM)
    return pl.pallas_call(
        functools.partial(kernel, n),
        out_shape=jax.ShapeDtypeStruct((rows, quarter), bf),
        in_specs=[hbm] * 10,
        out_specs=vm,
        scratch_shapes=[
            pltpu.VMEM(tokens.shape, bf),
            pltpu.VMEM((1, width), jnp.float32),
            pltpu.VMEM((top, rows), jnp.int32),
            pltpu.VMEM((top, rows), jnp.float32),
            pltpu.VMEM((width, 2 * hid), bf),
            pltpu.VMEM(down_proj.shape[1:], bf),
            pltpu.VMEM(shared_down.shape, bf),
            pltpu.VMEM((n * cap, rows), bf),
            pltpu.VMEM((top, nz, rows, 2 * cap), bf),
            pltpu.VMEM((n, cap, quarter), bf),
            pltpu.VMEM((4, n, cap, quarter), bf),
            pltpu.VMEM((4, 2, rows, depth), bf),
            pltpu.VMEM((4, 8, rows), jnp.float32),
            pltpu.VMEM((n, cap, 4 * hid), bf),
            pltpu.VMEM((rows, 4 * hid), bf),
            pltpu.VMEM((n, cap, quarter), bf),
            pltpu.VMEM((n, cap, quarter), bf),
            pltpu.VMEM((nz, depth, 2 * hid), bf),
            pltpu.VMEM((2 * rows, 2 * hid), jnp.float32),
            pltpu.VMEM((rows, 2 * hid), jnp.float32),
            pltpu.VMEM((rows, quarter), jnp.float32),
            dma((10,)),
            dma((n,)), dma((n,)),
            dma((nz, 2)), dma((nz, 2)),
            dma((nz, 2)), dma((nz, 2)),
            dma((nz,)), dma((nz,)),
            dma((6,)), dma((6,)),
            dma((4,)), dma((4,)),
            dma((nz, 4)), dma((nz, 4)),
            dma((4,)), dma((4,)),
            dma((n,)), dma((n,)),
            dma((5,)), dma((nz,)),
            dma, dma,
        ],
        compiler_params=pltpu.CompilerParams(
            collective_id=0, has_side_effects=True, vmem_limit_bytes=67043328
        ),
    )(tokens, norm_gain.reshape(1, width), expert_ids.T, expert_gates.T, gate_proj, up_proj, down_proj,
      shared_gate, shared_up, shared_down)


def solution(mesh):
    return jax.shard_map(
        functools.partial(shards, plain=not fits(mesh)),
        mesh=mesh,
        in_specs=(
            P("ep", "tp"),
            P(),
            P("ep", None),
            P("ep", None),
            P("ep", None, "tp"),
            P("ep", None, "tp"),
            P("ep", None, "tp"),
            P("ep", "tp"),
            P("ep", "tp"),
            P(None, "tp"),
        ),
        out_specs=P("ep", "tp"),
        check_vma=False,
    )
```

time: 66.3 us -> 79.2 us (1.19)
  Pallas kernels: 64.1 us -> 77.4 us
    pallas_call x1, Pallas kernels: 64.1 us -> 77.4 us  [shards(): pl.pallas_call(functools.partial(kernel, n), out_shape=jax.ShapeDtypeStru...]
where the time goes in v2:
time: 79.2 us; the launch traced here: 79 us
  Pallas kernels  77.4 us (98%)
  local copies, waits for them, and re-layouts  1.67 us (2%)
    pallas_call x1, Pallas kernels, shards(): pl.pallas_call(functools.partial(kernel, n), out_shape=jax.ShapeDtypeStru...  77.4 us
    unnamed x1, local copies, waits for them, and re-layouts  1.67 us

profile of v2, /device:TPU:0, one launch (start us, length us, event | category | flops | bytes accessed | tf_op | source)
XLA Modules:
  0.0 79.0 jit_solution(10400777241314860099)
XLA Ops:
  0.0 77.4 %shard_map.100 = bf16[128,1024]{1,0:T(8,128)(2,1)} custom-call(bf16[128,1024]{1,0:T(8,128)(2,1)} %tokens_hbm.1, f32[1,4096]{1,0:T(1,128)} %bitcast.3, s32[2,128]{1,0:T(2,128)} %bitcast.4, f32[2,128]{1,0:T(2,128)} %bitcast.5, bf16[1,4096,128]{2,1,0:T(8,128)(2,1)} %gate_w.1, bf16[1,4096,128]{2,1,0:T(8,128)(2,1)} %up_w.1, bf16[1,512,1024]{2,1,0:T(8,128)(2,1)} %down_w.1, ...), custom_call_target="tpu_custom_call" | custom-call | tf_op jit(solution)/shard_map/pallas_call | solution.py:419
  77.4 1.7 %copy.12 = bf16[128,1024]{1,0:T(8,128)(2,1)} copy(bf16[128,1024]{1,0:T(8,128)(2,1)} %shard_map.100) | data formatting | bytes 524288

commit v3 on v2

--- a/solution.py
+++ b/solution.py
@@ -94,7 +94,7 @@
     tokens_hbm, gain_hbm, ids_hbm, gates_hbm, gate_w, up_w, down_w, sgate_w, sup_w, sdown_w,
     out,
     tokens, gain, ids, gates, wgu, wdn, sdn, pick, back, outbox, xs, tk, ssq, hb, shb, ob, ret, sw,
-    acc, pin, mix,
+    acc, pout, pin, she, mix,
     load_sem, disp_s, disp_r, mate_s, mate_r, far_s, far_r, fwd_s, fwd_r,
     tk_s, tk_r, ssq_s, ssq_r, hid_s, hid_r, shid_s, shid_r, ret_s, ret_r, sw_s, sw_r, part_s, part_r,
 ):
@@ -114,7 +114,8 @@
 
     side = 1 - 2 * (z // 2)
     inner = ((z + 1) // 2) % 2
-    order = [z + side * (i - inner * (0, 0, 3, 1)[i]) for i in range(nz)]
+    half = ep + 2 * side * (1 - 2 * inner)
+    order = [z + side * (i - inner * (0, 2, 0, 2)[i]) for i in range(nz)]
 
     def load(src, dst, k):
         c = pltpu.make_async_copy(src, dst, load_sem.at[k])
@@ -141,6 +142,7 @@
         pl.semaphore_signal(barrier, inc=1, device_id=((ep + d) % n, tp), device_id_type=MESH)
     for d in range(1, 4):
         pl.semaphore_signal(barrier, inc=1, device_id=(ep, (tp + d) % 4), device_id_type=MESH)
+        pl.semaphore_signal(barrier, inc=1, device_id=(half, (tp + d) % 4), device_id_type=MESH)
 
     def column(row):
         return jnp.broadcast_to(row.astype(jnp.float32), (rows, rows)).T
@@ -177,9 +179,9 @@
         ).astype(jnp.bfloat16)
     own = tokens[...].astype(jnp.float32)
     sums = jnp.broadcast_to(jnp.sum(own * own, axis=-1, keepdims=True), (rows, 128)).T
-    ssq[tp] = sums[0:8, :]
-
-    pl.semaphore_wait(barrier, n - 1 + 3)
+    ssq[1 - inner, tp] = sums[0:8, :]
+
+    pl.semaphore_wait(barrier, n - 1 + 6)
 
     sends = []
 
@@ -195,34 +197,59 @@
     def dispatch(e):
         go(remote(outbox.at[e], xs.at[tp, ep], disp_s.at[e], disp_r.at[ep], e, tp))
 
+    def spread_block(i, j):
+        s = order[i] * 2 + (x + j) % 2
+        blk = xs.at[tp, s]
+        go(remote(blk, blk, far_s.at[i, j], far_r.at[i, j], ep, far))
+        go(remote(blk, blk, mate_s.at[i, j], mate_r.at[i, j], ep, mate))
+
+    def rows_of(i):
+        blk = sw.at[order[i]]
+        return remote(blk, blk, sw_s.at[i], sw_r.at[order[i]], ep + 2 * side, tp)
+
+    def at_inner(f):
+        pl.when(inner == 1)(f)
+
+    def at_edge(f):
+        pl.when(inner == 0)(f)
+
+    spread_block(0, 0)
     dispatch(ox)
     for i in range(1, nz):
         for j in range(2):
             dispatch(order[i] * 2 + (x + j) % 2)
+    for c in shared_in:
+        c.wait()
+    at_edge(lambda: rows_of(0).start())
 
     mine = tokens.at[:, pl.ds(pl.multiple_of(x * depth, depth), depth)]
     theirs = tokens.at[:, pl.ds(pl.multiple_of((1 - x) * depth, depth), depth)]
-    go(remote(mine, tk.at[tp, 0], tk_s.at[0], tk_r.at[0], ep, mate))
-    go(remote(mine, tk.at[tp, 0], tk_s.at[1], tk_r.at[1], ep, far))
-    go(remote(theirs, tk.at[tp, 1], tk_s.at[2], tk_r.at[2], ox, tp))
+    home = ep + 2 * side * (1 - inner)
+    home_ox = ox + 2 * side * (1 - inner)
+    edge = ep - 2 * side
+    plane = 1 - inner
+
+    def own_tokens():
+        return remote(mine, tk.at[1, tp, 0], tk_s.at[0, 0], tk_r.at[1, 0], home, tp)
+
+    go(remote(theirs, tk.at[plane, tp, 1], tk_s.at[0, 1], tk_r.at[plane, 1], home_ox, tp))
+    at_edge(lambda: own_tokens().start())
     for d in range(1, 4):
-        go(remote(ssq.at[tp], ssq.at[tp], ssq_s.at[d], ssq_r.at[d], ep, (tp + d) % 4))
-    tk[tp, 0] = mine[...]
-
-    def other_tokens():
-        landed(tk.at[tp, 1], tk_r.at[2])
-        go(remote(tk.at[tp, 1], tk.at[tp, 1], tk_s.at[3], tk_r.at[3], ep, mate))
-        go(remote(tk.at[tp, 1], tk.at[tp, 1], tk_s.at[4], tk_r.at[4], ep, far))
-
-    def pass_tokens():
-        landed(tk.at[far, 0], tk_r.at[1])
-        landed(tk.at[far, 1], tk_r.at[4])
-        go(remote(tk.at[far], tk.at[far], tk_s.at[5], tk_r.at[5], ep, mate))
-
-    def have_tokens():
-        landed(tk.at[mate, 0], tk_r.at[0])
-        landed(tk.at[mate, 1], tk_r.at[3])
-        landed(tk.at[diag], tk_r.at[5])
+        go(remote(ssq.at[plane, tp], ssq.at[plane, tp], ssq_s.at[d], ssq_r.at[plane, tp], home, (tp + d) % 4))
+
+    def own_square():
+        return remote(ssq.at[1, tp], ssq.at[1, tp], ssq_s.at[0], ssq_r.at[1, tp], home, tp)
+
+    at_edge(lambda: own_square().start())
+
+    def first_tokens(who, k):
+        return remote(mine, tk.at[0, tp, 0], tk_s.at[0, k], tk_r.at[0, k], ep, who)
+
+    @pl.when(inner == 1)
+    def _():
+        first_tokens(far, 2).start()
+        first_tokens(mate, 3).start()
+        tk[0, tp, 0] = mine[...]
 
     def pair(ref, k, i):
         return ref.at[k, pl.ds(order[i] * 2, 2)]
@@ -230,11 +257,9 @@
     def stage_a(i):
         for j in range(2):
             s = order[i] * 2 + (x + j) % 2
-            blk = xs.at[tp, s]
             if i > 0 or j > 0:
-                landed(blk, disp_r.at[s])
-            go(remote(blk, blk, far_s.at[i, j], far_r.at[i, j], ep, far))
-            go(remote(blk, blk, mate_s.at[i, j], mate_r.at[i, j], ep, mate))
+                landed(xs.at[tp, s], disp_r.at[s])
+                spread_block(i, j)
 
     def both(k, sem, i):
         for j in range(2):
@@ -280,49 +305,133 @@
         h = hb[pl.ds(zz * 2, 2)].reshape(2 * cap, 4 * hid)
         res = jnp.dot(h, wdn[...], preferred_element_type=jnp.float32).astype(jnp.bfloat16)
         ob[pl.ds(zz * 2, 2)] = res.reshape(2, cap, quarter)
-        for j in range(2):
-            s = zz * 2 + (x + j) % 2
-            if i == 0 and j == 0:
-                ret[ep] = ob[ep]
-            else:
-                go(remote(ob.at[s], ret.at[ep], ret_s.at[s], ret_r.at[ep], s, tp))
-
-    def rows_of(i, way, k):
-        blk = sw.at[order[i]]
-        return remote(blk, blk, sw_s.at[k], sw_r.at[order[i]], ep + 2 * way * side, tp)
-
-    chain = [(0, 1, 0), (0, -1, 1), (1, -1, 2), (2, 1, 3), (3, -1, 4)]
-
-    def rows_start(i):
+
+    def back_to(i, j):
+        s = order[i] * 2 + (x + j) % 2
+        return remote(ob.at[s], ret.at[ep], ret_s.at[s], ret_r.at[ep], s, tp)
+
+    backs = [[back_to(i, j) for j in range(i == 0, 2)] for i in range(nz)]
+
+    def send_back(i):
         if i == 0:
-            for c in shared_in:
-                c.wait()
-            rows_of(*chain[0]).start()
-
-            @pl.when(inner == 1)
-            def _():
-                rows_of(*chain[1]).start()
-        else:
-            landed(sw.at[order[i]], sw_r.at[order[i]])
-
-            @pl.when(inner == 1)
-            def _():
-                rows_of(*chain[i + 1]).start()
-
-    def rows_end():
-        rows_of(*chain[0]).wait_send()
-
+            ret[ep] = ob[ep]
+        for c in backs[i]:
+            c.start()
+
+    def rows_pass():
         @pl.when(inner == 1)
         def _():
-            for c in chain[1:]:
-                rows_of(*c).wait_send()
-
-    def shared_add(i):
-        zz = order[i]
-        cols = pl.ds(pl.multiple_of((2 * zz + x) * depth, depth), depth)
-        v = (tk[zz].reshape(2 * rows, depth).astype(jnp.float32) * gain[:, cols]).astype(jnp.bfloat16)
-        part = jnp.dot(v, sw[zz], preferred_element_type=jnp.float32)
-        acc[...] = part if i == 0 else acc[...] + part
+            landed(sw.at[order[1]], sw_r.at[order[1]])
+            rows_of(1).start()
+
+    def tokens_to(p, who, k):
+        blk = tk.at[1, tp] if p == 1 else tk.at[0, tp, 1]
+        return remote(blk, blk, tk_s.at[p, k], tk_r.at[p, k], ep, who)
+
+    def tokens_on(p):
+        return remote(tk.at[p, far], tk.at[p, far], tk_s.at[p, 4], tk_r.at[p, 4], ep, mate)
+
+    def spread_tokens(p):
+        if p == 1:
+            landed(tk.at[1, tp, 0], tk_r.at[1, 0])
+        landed(tk.at[p, tp, 1], tk_r.at[p, 1])
+        tokens_to(p, far, 5).start()
+        tokens_to(p, mate, 6).start()
+
+    def pass_tokens(p):
+        if p == 0:
+            landed(tk.at[0, far, 0], tk_r.at[0, 2])
+            landed(tk.at[0, far, 1], tk_r.at[0, 5])
+        else:
+            landed(tk.at[1, far], tk_r.at[1, 5])
+        tokens_on(p).start()
+
+    def partial(p):
+        return remote(pout.at[p], pin.at[p], part_s.at[p], part_r.at[p], ox, tp)
+
+    def shared_sum(p):
+        if p == 0:
+            landed(tk.at[0, mate, 0], tk_r.at[0, 3])
+            landed(tk.at[0, mate, 1], tk_r.at[0, 6])
+        else:
+            landed(tk.at[1, mate], tk_r.at[1, 6])
+        landed(tk.at[p, diag], tk_r.at[p, 4])
+        val = jnp.zeros((2 * rows, 2 * hid), jnp.float32)
+        for i in (0, 1, 3, 2):
+            zz = order[i]
+            if p == 1 and i in (2, 3):
+                landed(sw.at[zz], sw_r.at[zz])
+            cols = pl.ds(pl.multiple_of((2 * zz + x) * depth, depth), depth)
+            v = (tk[p, zz].reshape(2 * rows, depth).astype(jnp.float32) * gain[:, cols]).astype(jnp.bfloat16)
+            val = val + jnp.dot(v, sw[zz], preferred_element_type=jnp.float32)
+        acc[p] = val[0:rows, :]
+        pout[p] = val[rows:, :].astype(jnp.bfloat16)
+        partial(p).start()
+
+    at = pl.ds(pl.multiple_of(tp * hid, 128), hid)
+
+    def hidden_to(p, d):
+        frm = shb.at[:, at] if p == 0 else she
+        return remote(frm, shb.at[:, at], shid_s.at[p, d], shid_r.at[tp], ep if p == 0 else edge, (tp + d) % 4)
+
+    def shared_hidden(p):
+        square = jnp.zeros((8, rows), jnp.float32)
+        for k in range(4):
+            square = square + ssq[p, k]
+        scale = column(lax.rsqrt(square[0:1, :] / width + 1e-06))[:, 0:1]
+        landed(pin.at[p], part_r.at[p])
+        val = silu_mul((acc[p] + pin[p].astype(jnp.float32)) * scale, hid)
+        if p == 0:
+            shb[:, at] = val
+        else:
+            she[...] = val
+        for d in (2, 3, 1, 0):
+            if p == 1 or d > 0:
+                hidden_to(p, d).start()
+
+    def shared_inner():
+        @pl.when(inner == 1)
+        def _():
+            pass_tokens(1)
+            for d in range(1, 4):
+                landed(ssq.at[0, (tp + d) % 4], ssq_r.at[0, (tp + d) % 4])
+            for k in range(4):
+                landed(ssq.at[1, k], ssq_r.at[1, k])
+            shared_sum(1)
+            shared_sum(0)
+            shared_hidden(1)
+            shared_hidden(0)
+
+    def shared_end():
+        for d in range(1, 4):
+            frm = (tp + d) % 4
+            landed(shb.at[:, pl.ds(pl.multiple_of(frm * hid, 128), hid)], shid_r.at[frm])
+
+        @pl.when(inner == 0)
+        def _():
+            landed(shb.at[:, at], shid_r.at[tp])
+
+    def shared_drain():
+        rows_of(0).wait_send()
+
+        @pl.when(inner == 0)
+        def _():
+            own_tokens().wait_send()
+            own_square().wait_send()
+
+        @pl.when(inner == 1)
+        def _():
+            rows_of(1).wait_send()
+            first_tokens(far, 2).wait_send()
+            first_tokens(mate, 3).wait_send()
+            for p in range(2):
+                tokens_to(p, far, 5).wait_send()
+                tokens_to(p, mate, 6).wait_send()
+                tokens_on(p).wait_send()
+                partial(p).wait_send()
+                for d in range(4):
+                    if p == 1 or d > 0:
+                        hidden_to(p, d).wait_send()
 
     def combine(i):
         zz = order[i]
@@ -339,57 +448,42 @@
     stage_a(0)
     stage_a(1)
     stage_b(0)
-    other_tokens()
     stage_c(0)
     stage_b(1)
     stage_a(2)
-    rows_start(0)
+    stage_c(1)
+    at_inner(lambda: rows_of(0).start())
     stage_d(0)
-    stage_c(1)
-    stage_d(1)
+    send_back(0)
     stage_b(2)
     stage_a(3)
-    pass_tokens()
+    stage_d(1)
+    send_back(1)
+    rows_pass()
     stage_c(2)
-    rows_start(1)
+    at_inner(lambda: spread_tokens(0))
     stage_b(3)
     stage_d(2)
+    send_back(2)
     stage_c(3)
+    at_inner(lambda: spread_tokens(1))
+    at_inner(lambda: pass_tokens(0))
     stage_d(3)
-    have_tokens()
-    shared_add(0)
-    shared_add(1)
-    rows_start(2)
-    shared_add(2)
-    rows_start(3)
-    shared_add(3)
-    go(remote(acc.at[pl.ds(rows, rows)], pin, part_s, part_r, ox, tp))
-    square = ssq[tp]
-    for d in range(1, 4):
-        frm = (tp - d + 4) % 4
-        landed(ssq.at[frm], ssq_r.at[d])
-        square = square + ssq[frm]
-    scale = column(lax.rsqrt(square[0:1, :] / width + 1e-06))[:, 0:1]
+    send_back(3)
     mix[...] = jnp.zeros((rows, quarter), jnp.float32)
     gates_in.wait()
+    shared_inner()
     combine(0)
-    landed(pin, part_r)
-    at = pl.ds(pl.multiple_of(tp * hid, 128), hid)
-    shb[:, at] = silu_mul((acc[0:rows, :] + pin[...]) * scale, hid)
-    for d in (2, 1, 3):
-        go(remote(shb.at[:, at], shb.at[:, at], shid_s.at[d], shid_r.at[d], ep, (tp + d) % 4))
     combine(1)
     combine(2)
-    for d in range(1, 4):
-        frm = pl.ds(pl.multiple_of(((tp - d + 4) % 4) * hid, 128), hid)
-        landed(shb.at[:, frm], shid_r.at[d])
+    shared_end()
     sdown_in.wait()
     mix[...] += jnp.dot(shb[...], sdn[...], preferred_element_type=jnp.float32)
     combine(3)
     out[...] = mix[...].astype(jnp.bfloat16)
-    for c in sends:
+    for c in sends + sum(backs, []):
         c.wait_send()
-    rows_end()
+    shared_drain()
 
 
 def shards(
@@ -433,28 +527,30 @@
             pltpu.VMEM((top, nz, rows, 2 * cap), bf),
             pltpu.VMEM((n, cap, quarter), bf),
             pltpu.VMEM((4, n, cap, quarter), bf),
-            pltpu.VMEM((4, 2, rows, depth), bf),
-            pltpu.VMEM((4, 8, rows), jnp.float32),
+            pltpu.VMEM((2, 4, 2, rows, depth), bf),
+            pltpu.VMEM((2, 4, 8, rows), jnp.float32),
             pltpu.VMEM((n, cap, 4 * hid), bf),
             pltpu.VMEM((rows, 4 * hid), bf),
             pltpu.VMEM((n, cap, quarter), bf),
             pltpu.VMEM((n, cap, quarter), bf),
             pltpu.VMEM((nz, depth, 2 * hid), bf),
-            pltpu.VMEM((2 * rows, 2 * hid), jnp.float32),
-            pltpu.VMEM((rows, 2 * hid), jnp.float32),
+            pltpu.VMEM((2, rows, 2 * hid), jnp.float32),
+            pltpu.VMEM((2, rows, 2 * hid), bf),
+            pltpu.VMEM((2, rows, 2 * hid), bf),
+            pltpu.VMEM((rows, hid), bf),
             pltpu.VMEM((rows, quarter), jnp.float32),
             dma((10,)),
             dma((n,)), dma((n,)),
             dma((nz, 2)), dma((nz, 2)),
             dma((nz, 2)), dma((nz, 2)),
             dma((nz,)), dma((nz,)),
-            dma((6,)), dma((6,)),
-            dma((4,)), dma((4,)),
+            dma((2, 7)), dma((2, 7)),
+            dma((4,)), dma((2, 4)),
             dma((nz, 4)), dma((nz, 4)),
-            dma((4,)), dma((4,)),
+            dma((2, 4)), dma((4,)),
             dma((n,)), dma((n,)),
-            dma((5,)), dma((nz,)),
-            dma, dma,
+            dma((nz,)), dma((nz,)),
+            dma((2,)), dma((2,)),
         ],
         compiler_params=pltpu.CompilerParams(
             collective_id=0, has_side_effects=True, vmem_limit_bytes=67043328

time: 79.2 us -> 57.8 us (0.73)
  Pallas kernels: 77.4 us -> 55.8 us
    pallas_call x1, Pallas kernels: 77.4 us -> 55.8 us  [shards(): pl.pallas_call(functools.partial(kernel, n), out_shape=jax.ShapeDtypeStru...]
where the time goes in v3:
time: 57.8 us; the launch traced here: 57.5 us
  Pallas kernels  55.8 us (97%)
  local copies, waits for them, and re-layouts  1.67 us (3%)
    pallas_call x1, Pallas kernels, shards(): pl.pallas_call(functools.partial(kernel, n), out_shape=jax.ShapeDtypeStru...  55.8 us
    unnamed x1, local copies, waits for them, and re-layouts  1.67 us

profile of v3, /device:TPU:0, one launch (start us, length us, event | category | flops | bytes accessed | tf_op | source)
XLA Modules:
  0.0 57.5 jit_solution(3363552034982167212)
XLA Ops:
  0.0 55.8 %shard_map.100 = bf16[128,1024]{1,0:T(8,128)(2,1)} custom-call(bf16[128,1024]{1,0:T(8,128)(2,1)} %tokens_hbm.1, f32[1,4096]{1,0:T(1,128)} %bitcast.3, s32[2,128]{1,0:T(2,128)} %bitcast.4, f32[2,128]{1,0:T(2,128)} %bitcast.5, bf16[1,4096,128]{2,1,0:T(8,128)(2,1)} %gate_w.1, bf16[1,4096,128]{2,1,0:T(8,128)(2,1)} %up_w.1, bf16[1,512,1024]{2,1,0:T(8,128)(2,1)} %down_w.1, ...), custom_call_target="tpu_custom_call" | custom-call | tf_op jit(solution)/shard_map/pallas_call | solution.py:513
  55.8 1.7 %copy.12 = bf16[128,1024]{1,0:T(8,128)(2,1)} copy(bf16[128,1024]{1,0:T(8,128)(2,1)} %shard_map.100) | data formatting | bytes 524288

commit v4 on v3

--- a/solution.py
+++ b/solution.py
@@ -93,10 +93,9 @@
     n,
     tokens_hbm, gain_hbm, ids_hbm, gates_hbm, gate_w, up_w, down_w, sgate_w, sup_w, sdown_w,
     out,
-    tokens, gain, ids, gates, wgu, wdn, sdn, pick, back, outbox, xs, tk, ssq, hb, shb, ob, ret, sw,
+    tokens, gain, ids, gates, wgu, wdn, sdn, back, outbox, xs, tk, ssq, hb, shb, ob, ret, sw,
     acc, pout, pin, she, mix,
-    load_sem, disp_s, disp_r, mate_s, mate_r, far_s, far_r, fwd_s, fwd_r,
-    tk_s, tk_r, ssq_s, ssq_r, hid_s, hid_r, shid_s, shid_r, ret_s, ret_r, sw_s, sw_r, part_s, part_r,
+    load_sem, sent, disp_r, far_r, near_r, tk_r, ssq_r, hid_r, shid_r, ret_r, sw_r, part_r,
 ):
     ep, tp = lax.axis_index("ep"), lax.axis_index("tp")
     nz = n // 2
@@ -126,16 +125,12 @@
     tokens_in = load(tokens_hbm, tokens, 1)
     gates_in = load(gates_hbm, gates, 2)
     gain_in = load(gain_hbm, gain, 3)
-    shared_in = [
-        load(sgate_w, sw.at[z, :, pl.ds(0, hid)], 4),
-        load(sup_w, sw.at[z, :, pl.ds(hid, hid)], 5),
-    ]
-    expert_in = [
-        load(gate_w.at[0], wgu.at[:, pl.ds(0, hid)], 6),
-        load(up_w.at[0], wgu.at[:, pl.ds(hid, hid)], 7),
-    ]
-    down_in = load(down_w.at[0], wdn, 8)
-    sdown_in = load(sdown_w, sdn, 9)
+    load(sgate_w, sw.at[z, :, pl.ds(0, hid)], 4)
+    load(sup_w, sw.at[z, :, pl.ds(hid, hid)], 4)
+    load(gate_w.at[0], wgu.at[:, pl.ds(0, hid)], 5)
+    load(up_w.at[0], wgu.at[:, pl.ds(hid, hid)], 5)
+    down_in = load(down_w.at[0], wdn, 6)
+    sdown_in = load(sdown_w, sdn, 7)
 
     barrier = pltpu.get_barrier_semaphore()
     for d in range(1, n):
@@ -147,65 +142,49 @@
     def column(row):
         return jnp.broadcast_to(row.astype(jnp.float32), (rows, rows)).T
 
-    lane = lax.broadcasted_iota(jnp.int32, (rows, 128), 1).astype(jnp.float32)
     ids_in.wait()
-    named0 = (lane == column(ids[0:1, :])).astype(jnp.float32)
-    named1 = (lane == column(ids[1:2, :])).astype(jnp.float32)
-    named = (named0 + named1).astype(jnp.bfloat16)
-    before = (
-        lax.broadcasted_iota(jnp.int32, (rows, rows), 1) < lax.broadcasted_iota(jnp.int32, (rows, rows), 0)
-    ).astype(jnp.float32).astype(jnp.bfloat16)
-    place = jnp.dot(before, named, preferred_element_type=jnp.float32).astype(jnp.bfloat16)
-    low = lax.broadcasted_iota(jnp.int32, (128, slots), 0) * cap
-    col = lax.broadcasted_iota(jnp.int32, (128, slots), 1)
-    spread = ((col >= low) & (col < low + cap)).astype(jnp.float32).astype(jnp.bfloat16)
-    place_x = jnp.dot(place, spread, preferred_element_type=jnp.float32)
-    colf = lax.broadcasted_iota(jnp.int32, (rows, slots), 1).astype(jnp.float32)
-    within = colf - jnp.floor((colf + 0.5) / cap) * cap
-    hit = jnp.abs(place_x - within) < 0.5
-    total = jnp.zeros((rows, slots), jnp.float32)
-    for k, one in enumerate((named0, named1)):
-        sel = jnp.where(
-            hit, jnp.dot(one.astype(jnp.bfloat16), spread, preferred_element_type=jnp.float32), 0.0
-        )
-        for e in range(nz):
-            back[k, e] = sel[:, 2 * e * cap : 2 * (e + 1) * cap].astype(jnp.bfloat16)
-        total = total + sel
-    pick[...] = total.T.astype(jnp.bfloat16)
+    sub = lax.broadcasted_iota(jnp.int32, (rows, rows), 0)
+    tok = lax.broadcasted_iota(jnp.int32, (rows, rows), 1)
+    one = ((sub == ids[0:1, :]) | (sub == ids[1:2, :])).astype(jnp.float32).astype(jnp.bfloat16)
+    earlier = (sub < tok).astype(jnp.float32).astype(jnp.bfloat16)
+    place = jnp.dot(one, earlier, preferred_element_type=jnp.float32).astype(jnp.bfloat16)
+    slot = lax.broadcasted_iota(jnp.int32, (slots, rows), 0)
+    low = lax.broadcasted_iota(jnp.int32, (slots, rows), 1) * cap
+    spread = ((slot >= low) & (slot < low + cap)).astype(jnp.float32).astype(jnp.bfloat16)
+    place = jnp.dot(spread, place, preferred_element_type=jnp.float32)
+    one = jnp.dot(spread, one, preferred_element_type=jnp.float32)
+    slotf = slot.astype(jnp.float32)
+    within = slotf - jnp.floor((slotf + 0.5) / cap) * cap
+    pick = jnp.where(jnp.abs(place - within) < 0.5, one, 0.0).astype(jnp.bfloat16)
     tokens_in.wait()
-    for e in range(n):
-        outbox[e] = jnp.dot(
-            pick[e * cap : (e + 1) * cap, :], tokens[...], preferred_element_type=jnp.float32
-        ).astype(jnp.bfloat16)
-    own = tokens[...].astype(jnp.float32)
-    sums = jnp.broadcast_to(jnp.sum(own * own, axis=-1, keepdims=True), (rows, 128)).T
-    ssq[1 - inner, tp] = sums[0:8, :]
+    outbox[...] = (
+        jnp.dot(pick, tokens[...], preferred_element_type=jnp.float32)
+        .astype(jnp.bfloat16)
+        .reshape(n, cap, quarter)
+    )
 
     pl.semaphore_wait(barrier, n - 1 + 6)
-
-    sends = []
-
-    def go(c):
-        c.start()
-        sends.append(c)
 
     def landed(dst, sem):
         remote(dst, dst, sem, sem, ep, mate).wait_recv()
 
+    def gone(src, k):
+        remote(src, src, sent.at[k], sent.at[k], ep, mate).wait_send()
+
     xs[tp, ep] = outbox[ep]
 
     def dispatch(e):
-        go(remote(outbox.at[e], xs.at[tp, ep], disp_s.at[e], disp_r.at[ep], e, tp))
+        remote(outbox.at[e], xs.at[tp, ep], sent.at[0], disp_r.at[ep], e, tp).start()
 
     def spread_block(i, j):
         s = order[i] * 2 + (x + j) % 2
         blk = xs.at[tp, s]
-        go(remote(blk, blk, far_s.at[i, j], far_r.at[i, j], ep, far))
-        go(remote(blk, blk, mate_s.at[i, j], mate_r.at[i, j], ep, mate))
+        remote(blk, blk, sent.at[1], far_r.at[i], ep, far).start()
+        remote(blk, blk, sent.at[1], near_r.at[i], ep, mate).start()
 
     def rows_of(i):
         blk = sw.at[order[i]]
-        return remote(blk, blk, sw_s.at[i], sw_r.at[order[i]], ep + 2 * side, tp)
+        return remote(blk, blk, sent.at[9], sw_r.at[order[i]], ep + 2 * side, tp)
 
     def at_inner(f):
         pl.when(inner == 1)(f)
@@ -218,8 +197,7 @@
     for i in range(1, nz):
         for j in range(2):
             dispatch(order[i] * 2 + (x + j) % 2)
-    for c in shared_in:
-        c.wait()
+    pltpu.make_async_copy(sw.at[z], sw.at[z], load_sem.at[4]).wait()
     at_edge(lambda: rows_of(0).start())
 
     mine = tokens.at[:, pl.ds(pl.multiple_of(x * depth, depth), depth)]
@@ -230,26 +208,51 @@
     plane = 1 - inner
 
     def own_tokens():
-        return remote(mine, tk.at[1, tp, 0], tk_s.at[0, 0], tk_r.at[1, 0], home, tp)
-
-    go(remote(theirs, tk.at[plane, tp, 1], tk_s.at[0, 1], tk_r.at[plane, 1], home_ox, tp))
+        return remote(mine, tk.at[1, tp, 0], sent.at[4], tk_r.at[1], home, tp)
+
+    remote(theirs, tk.at[plane, tp, 1], sent.at[4], tk_r.at[plane], home_ox, tp).start()
     at_edge(lambda: own_tokens().start())
+    own = tokens[...].astype(jnp.float32)
+    sums = jnp.broadcast_to(jnp.sum(own * own, axis=-1, keepdims=True), (rows, 128)).T
+    ssq[plane, tp] = sums[0:8, :]
     for d in range(1, 4):
-        go(remote(ssq.at[plane, tp], ssq.at[plane, tp], ssq_s.at[d], ssq_r.at[plane, tp], home, (tp + d) % 4))
+        remote(ssq.at[plane, tp], ssq.at[plane, tp], sent.at[5], ssq_r.at[plane], home, (tp + d) % 4).start()
 
     def own_square():
-        return remote(ssq.at[1, tp], ssq.at[1, tp], ssq_s.at[0], ssq_r.at[1, tp], home, tp)
+        return remote(ssq.at[1, tp], ssq.at[1, tp], sent.at[5], ssq_r.at[1], home, tp)
 
     at_edge(lambda: own_square().start())
 
     def first_tokens(who, k):
-        return remote(mine, tk.at[0, tp, 0], tk_s.at[0, k], tk_r.at[0, k], ep, who)
+        return remote(mine, tk.at[0, tp, 0], sent.at[3], tk_r.at[k], ep, who)
 
     @pl.when(inner == 1)
     def _():
         first_tokens(far, 2).start()
-        first_tokens(mate, 3).start()
+        first_tokens(mate, 4).start()
         tk[0, tp, 0] = mine[...]
+
+    def places():
+        lane = lax.broadcasted_iota(jnp.int32, (rows, 128), 1).astype(jnp.float32)
+        ones = [(lane == column(ids[k : k + 1, :])).astype(jnp.float32) for k in range(2)]
+        named = (ones[0] + ones[1]).astype(jnp.bfloat16)
+        before = (tok < sub).astype(jnp.float32).astype(jnp.bfloat16)
+        place = jnp.dot(before, named, preferred_element_type=jnp.float32).astype(jnp.bfloat16)
+        low = lax.broadcasted_iota(jnp.int32, (128, slots), 0) * cap
+        col = lax.broadcasted_iota(jnp.int32, (128, slots), 1)
+        spread = ((col >= low) & (col < low + cap)).astype(jnp.float32).astype(jnp.bfloat16)
+        place = jnp.dot(place, spread, preferred_element_type=jnp.float32)
+        colf = lax.broadcasted_iota(jnp.int32, (rows, slots), 1).astype(jnp.float32)
+        within = colf - jnp.floor((colf + 0.5) / cap) * cap
+        hit = jnp.abs(place - within) < 0.5
+        for k in range(2):
+            sel = jnp.where(
+                hit, jnp.dot(ones[k].astype(jnp.bfloat16), spread, preferred_element_type=jnp.float32), 0.0
+            )
+            for e in range(nz):
+                back[k, e] = sel[:, 2 * e * cap : 2 * (e + 1) * cap].astype(jnp.bfloat16)
+
+    places()
 
     def pair(ref, k, i):
         return ref.at[k, pl.ds(order[i] * 2, 2)]
@@ -261,21 +264,15 @@
                 landed(xs.at[tp, s], disp_r.at[s])
                 spread_block(i, j)
 
-    def both(k, sem, i):
-        for j in range(2):
-            landed(xs.at[k, order[i] * 2 + (x + j) % 2], sem.at[i, j])
-
     def stage_b(i):
-        both(far, far_r, i)
         blk = pair(xs, far, i)
-        go(remote(blk, blk, fwd_s.at[i], fwd_r.at[i], ep, mate))
+        landed(blk, far_r.at[i])
+        remote(blk, blk, sent.at[1], near_r.at[i], ep, mate).start()
 
     def stage_c(i):
-        both(mate, mate_r, i)
-        landed(pair(xs, diag, i), fwd_r.at[i])
+        landed(xs.at[pl.ds(0, 2), pl.ds(0, 2)], near_r.at[i])
         if i == 0:
-            expert_in[0].wait()
-            expert_in[1].wait()
+            pltpu.make_async_copy(wgu, wgu, load_sem.at[5]).wait()
             gain_in.wait()
         zz = order[i]
         sq = jnp.zeros((2 * cap, 1), jnp.float32)
@@ -289,26 +286,23 @@
             v = xs[k, pl.ds(zz * 2, 2)].reshape(2 * cap, quarter).astype(jnp.float32)
             nk = (v * scale * gain[:, cols]).astype(jnp.bfloat16)
             val = val + jnp.dot(nk, wgu[cols, :], preferred_element_type=jnp.float32)
-        at = pl.ds(pl.multiple_of(tp * hid, 128), hid)
-        hb[pl.ds(zz * 2, 2), :, at] = silu_mul(val, hid).reshape(2, cap, hid)
+        hb[tp, pl.ds(zz * 2, 2)] = silu_mul(val, hid).reshape(2, cap, hid)
+        blk = pair(hb, tp, i)
         for d in (2, 1, 3):
-            blk = hb.at[pl.ds(zz * 2, 2), :, at]
-            go(remote(blk, blk, hid_s.at[i, d], hid_r.at[i, d], ep, (tp + d) % 4))
+            remote(blk, blk, sent.at[2], hid_r.at[i], ep, (tp + d) % 4).start()
 
     def stage_d(i):
         zz = order[i]
-        for d in range(1, 4):
-            at = pl.ds(pl.multiple_of(((tp - d + 4) % 4) * hid, 128), hid)
-            landed(hb.at[pl.ds(zz * 2, 2), :, at], hid_r.at[i, d])
+        landed(hb.at[pl.ds(0, 3), pl.ds(0, 2)], hid_r.at[i])
         if i == 0:
             down_in.wait()
-        h = hb[pl.ds(zz * 2, 2)].reshape(2 * cap, 4 * hid)
+        h = jnp.concatenate([hb[k, pl.ds(zz * 2, 2)].reshape(2 * cap, hid) for k in range(4)], axis=-1)
         res = jnp.dot(h, wdn[...], preferred_element_type=jnp.float32).astype(jnp.bfloat16)
         ob[pl.ds(zz * 2, 2)] = res.reshape(2, cap, quarter)
 
     def back_to(i, j):
         s = order[i] * 2 + (x + j) % 2
-        return remote(ob.at[s], ret.at[ep], ret_s.at[s], ret_r.at[ep], s, tp)
+        return remote(ob.at[s], ret.at[ep], sent.at[0], ret_r.at[z], s, tp)
 
     backs = [[back_to(i, j) for j in range(i == 0, 2)] for i in range(nz)]
 
@@ -326,36 +320,25 @@
 
     def tokens_to(p, who, k):
         blk = tk.at[1, tp] if p == 1 else tk.at[0, tp, 1]
-        return remote(blk, blk, tk_s.at[p, k], tk_r.at[p, k], ep, who)
+        return remote(blk, blk, sent.at[3], tk_r.at[k + p], ep, who)
 
     def tokens_on(p):
-        return remote(tk.at[p, far], tk.at[p, far], tk_s.at[p, 4], tk_r.at[p, 4], ep, mate)
+        return remote(tk.at[p, far], tk.at[p, far], sent.at[3], tk_r.at[4 + p], ep, mate)
 
     def spread_tokens(p):
-        if p == 1:
-            landed(tk.at[1, tp, 0], tk_r.at[1, 0])
-        landed(tk.at[p, tp, 1], tk_r.at[p, 1])
-        tokens_to(p, far, 5).start()
-        tokens_to(p, mate, 6).start()
+        landed(tk.at[1, tp] if p == 1 else tk.at[0, tp, 1], tk_r.at[p])
+        tokens_to(p, far, 2).start()
+        tokens_to(p, mate, 4).start()
 
     def pass_tokens(p):
-        if p == 0:
-            landed(tk.at[0, far, 0], tk_r.at[0, 2])
-            landed(tk.at[0, far, 1], tk_r.at[0, 5])
-        else:
-            landed(tk.at[1, far], tk_r.at[1, 5])
+        landed(tk.at[p, far], tk_r.at[2 + p])
         tokens_on(p).start()
 
     def partial(p):
-        return remote(pout.at[p], pin.at[p], part_s.at[p], part_r.at[p], ox, tp)
+        return remote(pout.at[p], pin.at[p], sent.at[6], part_r.at[p], ox, tp)
 
     def shared_sum(p):
-        if p == 0:
-            landed(tk.at[0, mate, 0], tk_r.at[0, 3])
-            landed(tk.at[0, mate, 1], tk_r.at[0, 6])
-        else:
-            landed(tk.at[1, mate], tk_r.at[1, 6])
-        landed(tk.at[p, diag], tk_r.at[p, 4])
+        landed(tk.at[p, pl.ds(0, 2)], tk_r.at[4 + p])
         val = jnp.zeros((2 * rows, 2 * hid), jnp.float32)
         for i in (0, 1, 3, 2):
             zz = order[i]
@@ -368,11 +351,9 @@
         pout[p] = val[rows:, :].astype(jnp.bfloat16)
         partial(p).start()
 
-    at = pl.ds(pl.multiple_of(tp * hid, 128), hid)
-
     def hidden_to(p, d):
-        frm = shb.at[:, at] if p == 0 else she
-        return remote(frm, shb.at[:, at], shid_s.at[p, d], shid_r.at[tp], ep if p == 0 else edge, (tp + d) % 4)
+        frm = shb.at[tp] if p == 0 else she
+        return remote(frm, shb.at[tp], sent.at[7 + p], shid_r, ep if p == 0 else edge, (tp + d) % 4)
 
     def shared_hidden(p):
         square = jnp.zeros((8, rows), jnp.float32)
@@ -382,7 +363,7 @@
         landed(pin.at[p], part_r.at[p])
         val = silu_mul((acc[p] + pin[p].astype(jnp.float32)) * scale, hid)
         if p == 0:
-            shb[:, at] = val
+            shb[tp] = val
         else:
             she[...] = val
         for d in (2, 3, 1, 0):
@@ -393,52 +374,41 @@
         @pl.when(inner == 1)
         def _():
             pass_tokens(1)
-            for d in range(1, 4):
-                landed(ssq.at[0, (tp + d) % 4], ssq_r.at[0, (tp + d) % 4])
-            for k in range(4):
-                landed(ssq.at[1, k], ssq_r.at[1, k])
+            landed(ssq.at[0, pl.ds(0, 3)], ssq_r.at[0])
+            landed(ssq.at[1], ssq_r.at[1])
             shared_sum(1)
             shared_sum(0)
             shared_hidden(1)
             shared_hidden(0)
 
     def shared_end():
-        for d in range(1, 4):
-            frm = (tp + d) % 4
-            landed(shb.at[:, pl.ds(pl.multiple_of(frm * hid, 128), hid)], shid_r.at[frm])
+        at_inner(lambda: landed(shb.at[pl.ds(0, 3)], shid_r))
+        at_edge(lambda: landed(shb, shid_r))
+
+    def drain():
+        gone(xs.at[pl.ds(0, 2), pl.ds(0, n - 1)], 0)
+        gone(xs.at[pl.ds(0, 3)], 1)
+        gone(hb.at[pl.ds(0, 3)], 2)
 
         @pl.when(inner == 0)
         def _():
-            landed(shb.at[:, at], shid_r.at[tp])
-
-    def shared_drain():
-        rows_of(0).wait_send()
-
-        @pl.when(inner == 0)
-        def _():
-            own_tokens().wait_send()
-            own_square().wait_send()
+            gone(tk.at[0, 0], 4)
+            gone(ssq.at[0], 5)
+            gone(sw.at[0], 9)
 
         @pl.when(inner == 1)
         def _():
-            rows_of(1).wait_send()
-            first_tokens(far, 2).wait_send()
-            first_tokens(mate, 3).wait_send()
-            for p in range(2):
-                tokens_to(p, far, 5).wait_send()
-                tokens_to(p, mate, 6).wait_send()
-                tokens_on(p).wait_send()
-                partial(p).wait_send()
-                for d in range(4):
-                    if p == 1 or d > 0:
-                        hidden_to(p, d).wait_send()
+            gone(tk.at[pl.ds(0, 2), pl.ds(0, 3)], 3)
+            gone(tk.at[0, 0, 0], 4)
+            gone(ssq.at[0, pl.ds(0, 3)], 5)
+            gone(pin, 6)
+            gone(shb.at[pl.ds(0, 3)], 7)
+            gone(shb, 8)
+            gone(sw.at[pl.ds(0, 2)], 9)
 
     def combine(i):
         zz = order[i]
-        for j in range(2):
-            s = zz * 2 + (x + j) % 2
-            if i > 0 or j > 0:
-                landed(ret.at[s], ret_r.at[s])
+        landed(ret.at[pl.ds(0, 2)] if i > 0 else ret.at[0], ret_r.at[zz])
         got = ret[pl.ds(zz * 2, 2)].reshape(2 * cap, quarter)
         for k in range(2):
             mix[...] += column(gates[k : k + 1, :])[:, 0:1] * jnp.dot(
@@ -478,12 +448,11 @@
     combine(2)
     shared_end()
     sdown_in.wait()
-    mix[...] += jnp.dot(shb[...], sdn[...], preferred_element_type=jnp.float32)
+    hidden = jnp.concatenate([shb[k] for k in range(4)], axis=-1)
+    mix[...] += jnp.dot(hidden, sdn[...], preferred_element_type=jnp.float32)
     combine(3)
     out[...] = mix[...].astype(jnp.bfloat16)
-    for c in sends + sum(backs, []):
-        c.wait_send()
-    shared_drain()
+    drain()
 
 
 def shards(
@@ -510,6 +479,10 @@
     dma = pltpu.SemaphoreType.DMA
     vm = pl.BlockSpec(memory_space=pltpu.VMEM)
     hbm = pl.BlockSpec(memory_space=pltpu.HBM)
+    operands = (
+        tokens, norm_gain.reshape(1, width), expert_ids.T, expert_gates.T, gate_proj, up_proj, down_proj,
+        shared_gate, shared_up, shared_down,
+    )
     return pl.pallas_call(
         functools.partial(kernel, n),
         out_shape=jax.ShapeDtypeStruct((rows, quarter), bf),
@@ -523,14 +496,13 @@
             pltpu.VMEM((width, 2 * hid), bf),
             pltpu.VMEM(down_proj.shape[1:], bf),
             pltpu.VMEM(shared_down.shape, bf),
-            pltpu.VMEM((n * cap, rows), bf),
             pltpu.VMEM((top, nz, rows, 2 * cap), bf),
             pltpu.VMEM((n, cap, quarter), bf),
             pltpu.VMEM((4, n, cap, quarter), bf),
             pltpu.VMEM((2, 4, 2, rows, depth), bf),
             pltpu.VMEM((2, 4, 8, rows), jnp.float32),
-            pltpu.VMEM((n, cap, 4 * hid), bf),
-            pltpu.VMEM((rows, 4 * hid), bf),
+            pltpu.VMEM((4, n, cap, hid), bf),
+            pltpu.VMEM((4, rows, hid), bf),
             pltpu.VMEM((n, cap, quarter), bf),
             pltpu.VMEM((n, cap, quarter), bf),
             pltpu.VMEM((nz, depth, 2 * hid), bf),
@@ -539,24 +511,13 @@
             pltpu.VMEM((2, rows, 2 * hid), bf),
             pltpu.VMEM((rows, hid), bf),
             pltpu.VMEM((rows, quarter), jnp.float32),
-            dma((10,)),
-            dma((n,)), dma((n,)),
-            dma((nz, 2)), dma((nz, 2)),
-            dma((nz, 2)), dma((nz, 2)),
-            dma((nz,)), dma((nz,)),
-            dma((2, 7)), dma((2, 7)),
-            dma((4,)), dma((2, 4)),
-            dma((nz, 4)), dma((nz, 4)),
-            dma((2, 4)), dma((4,)),
-            dma((n,)), dma((n,)),
-            dma((nz,)), dma((nz,)),
-            dma((2,)), dma((2,)),
+            dma((8,)), dma((10,)), dma((n,)),
+            dma((nz,)), dma((nz,)), dma((6,)), dma((2,)), dma((nz,)), dma, dma((nz,)), dma((nz,)), dma((2,)),
         ],
         compiler_params=pltpu.CompilerParams(
-            collective_id=0, has_side_effects=True, vmem_limit_bytes=67043328
+            collective_id=0, has_side_effects=True, vmem_limit_bytes=48 * 1024 * 1024
         ),
-    )(tokens, norm_gain.reshape(1, width), expert_ids.T, expert_gates.T, gate_proj, up_proj, down_proj,
-      shared_gate, shared_up, shared_down)
+    )(*(pltpu.with_memory_space_constraint(a, pltpu.HBM) for a in operands))
 
 
 def solution(mesh):

time: 57.8 us -> 55.2 us (0.955)
  Pallas kernels: 55.8 us -> 54 us
  local copies, waits for them, and re-layouts: 1.67 us -> 0.71 us
    pallas_call x1, Pallas kernels: 55.8 us -> 54 us  [shards(): pl.pallas_call(functools.partial(kernel, n), out_shape=jax.ShapeDtypeStru...]
    unnamed x1, local copies, waits for them, and re-layouts: 1.67 us -> 0.71 us
where the time goes in v4:
time: 55.2 us; the launch traced here: 54.7 us
  Pallas kernels  54 us (98%)
  local copies, waits for them, and re-layouts  0.71 us (1%)
    pallas_call x1, Pallas kernels, shards(): pl.pallas_call(functools.partial(kernel, n), out_shape=jax.ShapeDtypeStru...  54 us

profile of v4, /device:TPU:0, one launch (start us, length us, event | category | flops | bytes accessed | tf_op | source)
XLA Modules:
  0.0 54.7 jit_solution(10670536259858783255)
XLA Ops:
  0.0 54.0 %shard_map.100 = bf16[128,1024]{1,0:T(8,128)(2,1)S(1)} custom-call(bf16[128,1024]{1,0:T(8,128)(2,1)} %tokens_hbm.1, f32[1,4096]{1,0:T(1,128)} %bitcast.3, s32[2,128]{1,0:T(2,128)} %bitcast.4, f32[2,128]{1,0:T(2,128)} %bitcast.5, bf16[1,4096,128]{2,1,0:T(8,128)(2,1)} %gate_w.1, bf16[1,4096,128]{2,1,0:T(8,128)(2,1)} %up_w.1, bf16[1,512,1024]{2,1,0:T(8,128)(2,1)} %down_w.1, ...), custom_call_target="tpu_custom_call" | custom-call | tf_op jit(solution)/shard_map/pallas_call | solution.py:486
  54.0 0.7 %copy.12 = bf16[128,1024]{1,0:T(8,128)(2,1)} copy(bf16[128,1024]{1,0:T(8,128)(2,1)S(1)} %shard_map.100) | data formatting | bytes 524288

commit v5 on v4

--- a/solution.py
+++ b/solution.py
@@ -208,7 +208,7 @@
     plane = 1 - inner
 
     def own_tokens():
-        return remote(mine, tk.at[1, tp, 0], sent.at[4], tk_r.at[1], home, tp)
+        return remote(mine, tk.at[1, tp, 0], sent.at[4], tk_r.at[6], home, tp)
 
     remote(theirs, tk.at[plane, tp, 1], sent.at[4], tk_r.at[plane], home_ox, tp).start()
     at_edge(lambda: own_tokens().start())
@@ -318,17 +318,17 @@
             landed(sw.at[order[1]], sw_r.at[order[1]])
             rows_of(1).start()
 
-    def tokens_to(p, who, k):
-        blk = tk.at[1, tp] if p == 1 else tk.at[0, tp, 1]
+    def tokens_to(p, b, who, k):
+        blk = tk.at[p, tp, b]
         return remote(blk, blk, sent.at[3], tk_r.at[k + p], ep, who)
 
     def tokens_on(p):
         return remote(tk.at[p, far], tk.at[p, far], sent.at[3], tk_r.at[4 + p], ep, mate)
 
-    def spread_tokens(p):
-        landed(tk.at[1, tp] if p == 1 else tk.at[0, tp, 1], tk_r.at[p])
-        tokens_to(p, far, 2).start()
-        tokens_to(p, mate, 4).start()
+    def spread_tokens(p, b):
+        landed(tk.at[p, tp, b], tk_r.at[p if b == 1 else 6])
+        tokens_to(p, b, far, 2).start()
+        tokens_to(p, b, mate, 4).start()
 
     def pass_tokens(p):
         landed(tk.at[p, far], tk_r.at[2 + p])
@@ -353,7 +353,7 @@
 
     def hidden_to(p, d):
         frm = shb.at[tp] if p == 0 else she
-        return remote(frm, shb.at[tp], sent.at[7 + p], shid_r, ep if p == 0 else edge, (tp + d) % 4)
+        return remote(frm, shb.at[tp], sent.at[7 + p], shid_r.at[0], ep if p == 0 else edge, (tp + d) % 4)
 
     def shared_hidden(p):
         square = jnp.zeros((8, rows), jnp.float32)
@@ -366,9 +366,8 @@
             shb[tp] = val
         else:
             she[...] = val
-        for d in (2, 3, 1, 0):
-            if p == 1 or d > 0:
-                hidden_to(p, d).start()
+        for d in (2, 3, 1) if p == 0 else (2, 0):
+            hidden_to(p, d).start()
 
     def shared_inner():
         @pl.when(inner == 1)
@@ -382,8 +381,14 @@
             shared_hidden(0)
 
     def shared_end():
-        at_inner(lambda: landed(shb.at[pl.ds(0, 3)], shid_r))
-        at_edge(lambda: landed(shb, shid_r))
+        at_inner(lambda: landed(shb.at[pl.ds(0, 3)], shid_r.at[0]))
+
+        @pl.when(inner == 0)
+        def _():
+            landed(shb.at[pl.ds(0, 2)], shid_r.at[0])
+            for k in (tp, far):
+                remote(shb.at[k], shb.at[k], sent.at[7], shid_r.at[1], ep, mate).start()
+            landed(shb.at[pl.ds(0, 2)], shid_r.at[1])
 
     def drain():
         gone(xs.at[pl.ds(0, 2), pl.ds(0, n - 1)], 0)
@@ -394,6 +399,7 @@
         def _():
             gone(tk.at[0, 0], 4)
             gone(ssq.at[0], 5)
+            gone(shb.at[pl.ds(0, 2)], 7)
             gone(sw.at[0], 9)
 
         @pl.when(inner == 1)
@@ -403,7 +409,7 @@
             gone(ssq.at[0, pl.ds(0, 3)], 5)
             gone(pin, 6)
             gone(shb.at[pl.ds(0, 3)], 7)
-            gone(shb, 8)
+            gone(shb.at[pl.ds(0, 2)], 8)
             gone(sw.at[pl.ds(0, 2)], 9)
 
     def combine(i):
@@ -431,12 +437,13 @@
     send_back(1)
     rows_pass()
     stage_c(2)
-    at_inner(lambda: spread_tokens(0))
+    at_inner(lambda: spread_tokens(0, 1))
     stage_b(3)
+    at_inner(lambda: spread_tokens(1, 1))
     stage_d(2)
     send_back(2)
     stage_c(3)
-    at_inner(lambda: spread_tokens(1))
+    at_inner(lambda: spread_tokens(1, 0))
     at_inner(lambda: pass_tokens(0))
     stage_d(3)
     send_back(3)
@@ -512,7 +519,7 @@
             pltpu.VMEM((rows, hid), bf),
             pltpu.VMEM((rows, quarter), jnp.float32),
             dma((8,)), dma((10,)), dma((n,)),
-            dma((nz,)), dma((nz,)), dma((6,)), dma((2,)), dma((nz,)), dma, dma((nz,)), dma((nz,)), dma((2,)),
+            dma((nz,)), dma((nz,)), dma((7,)), dma((2,)), dma((nz,)), dma((2,)), dma((nz,)), dma((nz,)), dma((2,)),
         ],
         compiler_params=pltpu.CompilerParams(
             collective_id=0, has_side_effects=True, vmem_limit_bytes=48 * 1024 * 1024

time: 55.2 us -> 54.1 us (0.980)
  Pallas kernels: 54 us -> 53.1 us
    pallas_call x1, Pallas kernels: 54 us -> 53.1 us  [shards(): pl.pallas_call(functools.partial(kernel, n), out_shape=jax.ShapeDtypeStru...]
where the time goes in v5:
time: 54.1 us; the launch traced here: 53.9 us
  Pallas kernels  53.1 us (98%)
  local copies, waits for them, and re-layouts  0.71 us (1%)
    pallas_call x1, Pallas kernels, shards(): pl.pallas_call(functools.partial(kernel, n), out_shape=jax.ShapeDtypeStru...  53.1 us

profile of v5, /device:TPU:0, one launch (start us, length us, event | category | flops | bytes accessed | tf_op | source)
XLA Modules:
  0.0 53.9 jit_solution(9299190806058657121)
XLA Ops:
  0.0 53.1 %shard_map.100 = bf16[128,1024]{1,0:T(8,128)(2,1)S(1)} custom-call(bf16[128,1024]{1,0:T(8,128)(2,1)} %tokens_hbm.1, f32[1,4096]{1,0:T(1,128)} %bitcast.3, s32[2,128]{1,0:T(2,128)} %bitcast.4, f32[2,128]{1,0:T(2,128)} %bitcast.5, bf16[1,4096,128]{2,1,0:T(8,128)(2,1)} %gate_w.1, bf16[1,4096,128]{2,1,0:T(8,128)(2,1)} %up_w.1, bf16[1,512,1024]{2,1,0:T(8,128)(2,1)} %down_w.1, ...), custom_call_target="tpu_custom_call" | custom-call | tf_op jit(solution)/shard_map/pallas_call | solution.py:493
  53.1 0.7 %copy.12 = bf16[128,1024]{1,0:T(8,128)(2,1)} copy(bf16[128,1024]{1,0:T(8,128)(2,1)S(1)} %shard_map.100) | data formatting | bytes 524288

commit v6 on v5

--- a/solution.py
+++ b/solution.py
@@ -95,7 +95,7 @@
     out,
     tokens, gain, ids, gates, wgu, wdn, sdn, back, outbox, xs, tk, ssq, hb, shb, ob, ret, sw,
     acc, pout, pin, she, mix,
-    load_sem, sent, disp_r, far_r, near_r, tk_r, ssq_r, hid_r, shid_r, ret_r, sw_r, part_r,
+    load_sem, sent, disp_r, far_r, near_r, tk_r, ssq_r, hid_r, hid_far, shid_r, ret_r, sw_r, part_r,
 ):
     ep, tp = lax.axis_index("ep"), lax.axis_index("tp")
     nz = n // 2
@@ -269,6 +269,8 @@
         landed(blk, far_r.at[i])
         remote(blk, blk, sent.at[1], near_r.at[i], ep, mate).start()
 
+    via = (0, 1)
+
     def stage_c(i):
         landed(xs.at[pl.ds(0, 2), pl.ds(0, 2)], near_r.at[i])
         if i == 0:
@@ -288,12 +290,22 @@
             val = val + jnp.dot(nk, wgu[cols, :], preferred_element_type=jnp.float32)
         hb[tp, pl.ds(zz * 2, 2)] = silu_mul(val, hid).reshape(2, cap, hid)
         blk = pair(hb, tp, i)
-        for d in (2, 1, 3):
-            remote(blk, blk, sent.at[2], hid_r.at[i], ep, (tp + d) % 4).start()
+        if i in via:
+            remote(blk, blk, sent.at[2], hid_far.at[i], ep, far).start()
+            remote(blk, blk, sent.at[2], hid_r.at[i], ep, mate).start()
+        else:
+            for d in (2, 1, 3):
+                remote(blk, blk, sent.at[2], hid_r.at[i], ep, (tp + d) % 4).start()
+
+    def hidden_on(i):
+        if i in via:
+            blk = pair(hb, far, i)
+            landed(blk, hid_far.at[i])
+            remote(blk, blk, sent.at[2], hid_r.at[i], ep, mate).start()
 
     def stage_d(i):
         zz = order[i]
-        landed(hb.at[pl.ds(0, 3), pl.ds(0, 2)], hid_r.at[i])
+        landed(hb.at[pl.ds(0, 2 if i in via else 3), pl.ds(0, 2)], hid_r.at[i])
         if i == 0:
             down_in.wait()
         h = jnp.concatenate([hb[k, pl.ds(zz * 2, 2)].reshape(2 * cap, hid) for k in range(4)], axis=-1)
@@ -376,6 +388,8 @@
             landed(ssq.at[0, pl.ds(0, 3)], ssq_r.at[0])
             landed(ssq.at[1], ssq_r.at[1])
             shared_sum(1)
+            send_back(3)
+            pass_tokens(0)
             shared_sum(0)
             shared_hidden(1)
             shared_hidden(0)
@@ -427,26 +441,27 @@
     stage_c(0)
     stage_b(1)
     stage_a(2)
+    hidden_on(0)
     stage_c(1)
     at_inner(lambda: rows_of(0).start())
     stage_d(0)
     send_back(0)
     stage_b(2)
+    hidden_on(1)
     stage_a(3)
     stage_d(1)
     send_back(1)
     rows_pass()
     stage_c(2)
-    at_inner(lambda: spread_tokens(0, 1))
     stage_b(3)
     at_inner(lambda: spread_tokens(1, 1))
+    at_inner(lambda: spread_tokens(0, 1))
     stage_d(2)
     send_back(2)
     stage_c(3)
     at_inner(lambda: spread_tokens(1, 0))
-    at_inner(lambda: pass_tokens(0))
     stage_d(3)
-    send_back(3)
+    at_edge(lambda: send_back(3))
     mix[...] = jnp.zeros((rows, quarter), jnp.float32)
     gates_in.wait()
     shared_inner()
@@ -519,7 +534,7 @@
             pltpu.VMEM((rows, hid), bf),
             pltpu.VMEM((rows, quarter), jnp.float32),
             dma((8,)), dma((10,)), dma((n,)),
-            dma((nz,)), dma((nz,)), dma((7,)), dma((2,)), dma((nz,)), dma((2,)), dma((nz,)), dma((nz,)), dma((2,)),
+            dma((nz,)), dma((nz,)), dma((7,)), dma((2,)), dma((nz,)), dma((nz,)), dma((2,)), dma((nz,)), dma((nz,)), dma((2,)),
         ],
         compiler_params=pltpu.CompilerParams(
             collective_id=0, has_side_effects=True, vmem_limit_bytes=48 * 1024 * 1024

time: 54.1 us -> 53.2 us (0.983)
  Pallas kernels: 53.1 us -> 52.2 us
    pallas_call x1, Pallas kernels: 53.1 us -> 52.2 us  [shards(): pl.pallas_call(functools.partial(kernel, n), out_shape=jax.ShapeDtypeStru...]
where the time goes in v6:
time: 53.2 us; the launch traced here: 52.9 us
  Pallas kernels  52.2 us (98%)
  local copies, waits for them, and re-layouts  0.71 us (1%)
    pallas_call x1, Pallas kernels, shards(): pl.pallas_call(functools.partial(kernel, n), out_shape=jax.ShapeDtypeStru...  52.2 us

profile of v6, /device:TPU:0, one launch (start us, length us, event | category | flops | bytes accessed | tf_op | source)
XLA Modules:
  0.0 52.9 jit_solution(11588259916067120914)
XLA Ops:
  0.0 52.2 %shard_map.100 = bf16[128,1024]{1,0:T(8,128)(2,1)S(1)} custom-call(bf16[128,1024]{1,0:T(8,128)(2,1)} %tokens_hbm.1, f32[1,4096]{1,0:T(1,128)} %bitcast.3, s32[2,128]{1,0:T(2,128)} %bitcast.4, f32[2,128]{1,0:T(2,128)} %bitcast.5, bf16[1,4096,128]{2,1,0:T(8,128)(2,1)} %gate_w.1, bf16[1,4096,128]{2,1,0:T(8,128)(2,1)} %up_w.1, bf16[1,512,1024]{2,1,0:T(8,128)(2,1)} %down_w.1, ...), custom_call_target="tpu_custom_call" | custom-call | tf_op jit(solution)/shard_map/pallas_call | solution.py:508
  52.2 0.7 %copy.12 = bf16[128,1024]{1,0:T(8,128)(2,1)} copy(bf16[128,1024]{1,0:T(8,128)(2,1)S(1)} %shard_map.100) | data formatting | bytes 524288

commit v7 on v6

--- a/solution.py
+++ b/solution.py
@@ -208,10 +208,18 @@
     plane = 1 - inner
 
     def own_tokens():
-        return remote(mine, tk.at[1, tp, 0], sent.at[4], tk_r.at[6], home, tp)
+        remote(mine, tk.at[1, tp, 0], sent.at[4], tk_r.at[0], ep, far).start()
+        remote(mine, tk.at[1, tp, 0], sent.at[4], tk_r.at[6], home, tp).start()
+
+    def edge_pass():
+        @pl.when(inner == 0)
+        def _():
+            blk = tk.at[1, far, 0]
+            landed(blk, tk_r.at[0])
+            remote(blk, blk, sent.at[4], tk_r.at[3], home, tp).start()
 
     remote(theirs, tk.at[plane, tp, 1], sent.at[4], tk_r.at[plane], home_ox, tp).start()
-    at_edge(lambda: own_tokens().start())
+    at_edge(own_tokens)
     own = tokens[...].astype(jnp.float32)
     sums = jnp.broadcast_to(jnp.sum(own * own, axis=-1, keepdims=True), (rows, 128)).T
     ssq[plane, tp] = sums[0:8, :]
@@ -224,7 +232,7 @@
     at_edge(lambda: own_square().start())
 
     def first_tokens(who, k):
-        return remote(mine, tk.at[0, tp, 0], sent.at[3], tk_r.at[k], ep, who)
+        return remote(mine, tk.at[0, tp, 0], sent.at[4], tk_r.at[k], ep, who)
 
     @pl.when(inner == 1)
     def _():
@@ -332,14 +340,15 @@
 
     def tokens_to(p, b, who, k):
         blk = tk.at[p, tp, b]
-        return remote(blk, blk, sent.at[3], tk_r.at[k + p], ep, who)
+        return remote(blk, blk, sent.at[3 if (p, b) != (1, 0) else 4], tk_r.at[k + p], ep, who)
 
     def tokens_on(p):
         return remote(tk.at[p, far], tk.at[p, far], sent.at[3], tk_r.at[4 + p], ep, mate)
 
     def spread_tokens(p, b):
         landed(tk.at[p, tp, b], tk_r.at[p if b == 1 else 6])
-        tokens_to(p, b, far, 2).start()
+        if (p, b) != (1, 0):
+            tokens_to(p, b, far, 2).start()
         tokens_to(p, b, mate, 4).start()
 
     def pass_tokens(p):
@@ -388,55 +397,60 @@
             landed(ssq.at[0, pl.ds(0, 3)], ssq_r.at[0])
             landed(ssq.at[1], ssq_r.at[1])
             shared_sum(1)
-            send_back(3)
             pass_tokens(0)
             shared_sum(0)
             shared_hidden(1)
             shared_hidden(0)
 
-    def shared_end():
-        at_inner(lambda: landed(shb.at[pl.ds(0, 3)], shid_r.at[0]))
-
+    def shared_swap():
         @pl.when(inner == 0)
         def _():
             landed(shb.at[pl.ds(0, 2)], shid_r.at[0])
             for k in (tp, far):
                 remote(shb.at[k], shb.at[k], sent.at[7], shid_r.at[1], ep, mate).start()
-            landed(shb.at[pl.ds(0, 2)], shid_r.at[1])
+
+    def shared_end():
+        at_inner(lambda: landed(shb.at[pl.ds(0, 3)], shid_r.at[0]))
+        at_edge(lambda: landed(shb.at[pl.ds(0, 2)], shid_r.at[1]))
 
     def drain():
         gone(xs.at[pl.ds(0, 2), pl.ds(0, n - 1)], 0)
         gone(xs.at[pl.ds(0, 3)], 1)
         gone(hb.at[pl.ds(0, 3)], 2)
+        gone(tk.at[0, pl.ds(0, 2)], 4)
 
         @pl.when(inner == 0)
         def _():
-            gone(tk.at[0, 0], 4)
             gone(ssq.at[0], 5)
             gone(shb.at[pl.ds(0, 2)], 7)
             gone(sw.at[0], 9)
 
         @pl.when(inner == 1)
         def _():
-            gone(tk.at[pl.ds(0, 2), pl.ds(0, 3)], 3)
-            gone(tk.at[0, 0, 0], 4)
+            gone(tk.at[0], 3)
             gone(ssq.at[0, pl.ds(0, 3)], 5)
             gone(pin, 6)
             gone(shb.at[pl.ds(0, 3)], 7)
             gone(shb.at[pl.ds(0, 2)], 8)
             gone(sw.at[pl.ds(0, 2)], 9)
 
-    def combine(i):
+    def combined(i):
         zz = order[i]
         landed(ret.at[pl.ds(0, 2)] if i > 0 else ret.at[0], ret_r.at[zz])
         got = ret[pl.ds(zz * 2, 2)].reshape(2 * cap, quarter)
+        val = 0.0 if i == 0 else mix[...]
         for k in range(2):
-            mix[...] += column(gates[k : k + 1, :])[:, 0:1] * jnp.dot(
+            val = val + column(gates[k : k + 1, :])[:, 0:1] * jnp.dot(
                 back[k, zz], got, preferred_element_type=jnp.float32
             )
+        return val
+
+    def combine(i):
+        mix[...] = combined(i)
 
     stage_a(0)
     stage_a(1)
+    edge_pass()
     stage_b(0)
     stage_c(0)
     stage_b(1)
@@ -461,19 +475,18 @@
     stage_c(3)
     at_inner(lambda: spread_tokens(1, 0))
     stage_d(3)
-    at_edge(lambda: send_back(3))
-    mix[...] = jnp.zeros((rows, quarter), jnp.float32)
+    send_back(3)
     gates_in.wait()
     shared_inner()
     combine(0)
     combine(1)
+    shared_swap()
     combine(2)
     shared_end()
     sdown_in.wait()
     hidden = jnp.concatenate([shb[k] for k in range(4)], axis=-1)
     mix[...] += jnp.dot(hidden, sdn[...], preferred_element_type=jnp.float32)
-    combine(3)
-    out[...] = mix[...].astype(jnp.bfloat16)
+    out[...] = combined(3).astype(jnp.bfloat16)
     drain()
 
 

time: 53.2 us -> 53.3 us (level)
  no operation moved by 1% of the time
where the time goes in v7:
time: 53.3 us; the launch traced here: 53 us
  Pallas kernels  52.3 us (98%)
  local copies, waits for them, and re-layouts  0.71 us (1%)
    pallas_call x1, Pallas kernels, shards(): pl.pallas_call(functools.partial(kernel, n), out_shape=jax.ShapeDtypeStru...  52.3 us

profile of v7, /device:TPU:0, one launch (start us, length us, event | category | flops | bytes accessed | tf_op | source)
XLA Modules:
  0.0 53.0 jit_solution(16170860502700267098)
XLA Ops:
  0.0 52.3 %shard_map.100 = bf16[128,1024]{1,0:T(8,128)(2,1)S(1)} custom-call(bf16[128,1024]{1,0:T(8,128)(2,1)} %tokens_hbm.1, f32[1,4096]{1,0:T(1,128)} %bitcast.3, s32[2,128]{1,0:T(2,128)} %bitcast.4, f32[2,128]{1,0:T(2,128)} %bitcast.5, bf16[1,4096,128]{2,1,0:T(8,128)(2,1)} %gate_w.1, bf16[1,4096,128]{2,1,0:T(8,128)(2,1)} %up_w.1, bf16[1,512,1024]{2,1,0:T(8,128)(2,1)} %down_w.1, ...), custom_call_target="tpu_custom_call" | custom-call | tf_op jit(solution)/shard_map/pallas_call | solution.py:521
  52.3 0.7 %copy.12 = bf16[128,1024]{1,0:T(8,128)(2,1)} copy(bf16[128,1024]{1,0:T(8,128)(2,1)S(1)} %shard_map.100) | data formatting | bytes 524288
